TPU v7x, 32 devices: a whole 2x2x4 slice. The times are simulated.
32 devices in a mesh: sp: 8 (over z, y), tp: 4 (over x, core).
Axes of the slice: x: 2, y: 2, z: 4, core: 2. Of those that a mesh axis runs over, the one named last changes fastest.
Arguments:
- tokens: bfloat16 [2048, 2048], P(('sp', 'tp')), may hold values from -6 to 6
- norm_gain: float32 [2048], replicated, may hold values from 0.1 to 1.9
- query_weight: bfloat16 [1024, 2048], P('tp', 'sp'), may hold values from -0.088609319 to 0.088609319
- key_weight: bfloat16 [256, 2048], P('tp', 'sp'), may hold values from -0.10628699 to 0.10628699
- value_weight: bfloat16 [256, 2048], P('tp', 'sp'), may hold values from -0.125 to 0.125
- gate_weight: bfloat16 [1024, 2048], P('tp', 'sp'), may hold values from -0.125 to 0.125
- left_weight: bfloat16 [1024, 2048], P('tp', 'sp'), may hold values from -0.125 to 0.125
- input_weight: bfloat16 [1024, 2048], P('tp', 'sp'), may hold values from -0.125 to 0.125
- query_gain: float32 [64], replicated, may hold values from 0.3 to 4.5, as said below
- key_gain: float32 [64], replicated, may hold values from 0.3 to 4.5, as said below
- sink_logit: float32 [16], P('tp'), may hold values from 2 to 7
- conv_weight: float32 [3, 1024], P(None, 'tp'), may hold values from -3 to 3
- out_attention: bfloat16 [1024, 2048], P('tp', 'sp'), may hold values from -0.125 to 0.125
- out_conv: bfloat16 [1024, 2048], P('tp', 'sp'), may hold values from -0.125 to 0.125
Outputs:
- mixed: bfloat16 [2048, 2048], P(('sp', 'tp'))
Inputs may be any that keep to these rules, and one draw needn't show every extreme that they name: `query_gain`: positive. `key_gain`: positive.
All inputs are finite; a program needn't handle non-finite values.
Results may differ from a plain program's by a relative error of at most 0.024.
Values may be sent and summed in bfloat16 or wider, within the bound.
A program may use at most 64 MiB of HBM per device.

v0:
```python
import functools

import jax
import jax.numpy as jnp
import numpy as np
from jax import lax
from jax.experimental import pallas as pl
from jax.experimental.pallas import tpu as pltpu
from jax.sharding import PartitionSpec as P

HEAD_DIM = 64
WINDOW = 128
BLOCK = 128


EPS = 1e-06
ROPE_BASE = 10000.0
NEG_FILL = -1e30


def with_halo(cells, sides, width):
    for axis, dim in sides:
        count = lax.axis_size(axis)
        ends = count - 1
        head = lax.slice_in_dim(cells, 0, width, axis=dim)
        tail = lax.slice_in_dim(cells, cells.shape[dim] - width, cells.shape[dim], axis=dim)
        cells = jnp.concatenate(
            [
                lax.ppermute(tail, axis, [(i, (i + 1) % count) for i in range(ends)]),
                cells,
                lax.ppermute(head, axis, [((i + 1) % count, i) for i in range(ends)]),
            ],
            axis=dim,
        )
    return cells


def normalize(values, gain):
    return values * lax.rsqrt(jnp.mean(values * values, axis=-1, keepdims=True) + EPS) * gain


def rotate(values, positions):
    half = values.shape[-1] // 2
    freq = ROPE_BASE ** (-jnp.arange(half, dtype=jnp.float32) / half)
    angle = positions[:, None] * freq
    cosine = jnp.cos(angle)[:, None, :]
    sine = jnp.sin(angle)[:, None, :]
    first = values[..., :half]
    second = values[..., half:]
    return jnp.concatenate(
        [first * cosine - second * sine, second * cosine + first * sine], axis=-1
    )


def project(rows, weight):
    return lax.dot_general(
        rows, weight, (((1,), (1,)), ((), ())), preferred_element_type=jnp.float32
    ).astype(jnp.bfloat16)


def attend(query_rot, key_rim, value_rim, sinks, offset, total):
    count = query_rot.shape[0]
    local_heads = query_rot.shape[1]
    kv_local = key_rim.shape[1]
    group = local_heads // kv_local
    span = BLOCK + 2 * WINDOW
    nblocks = count // BLOCK
    shaped = query_rot.reshape(nblocks, BLOCK, kv_local, group, HEAD_DIM)
    sink_group = sinks.reshape(kv_local, group)[:, :, None]

    def one_block(packed):
        block_index, query_block = packed
        begin = block_index * BLOCK
        key_block = lax.dynamic_slice_in_dim(key_rim, begin, span, 0)
        value_block = lax.dynamic_slice_in_dim(value_rim, begin, span, 0)
        scores = jnp.einsum(
            "qkgd,nkd->kgqn", query_block, key_block, preferred_element_type=jnp.float32
        ) * HEAD_DIM ** (-0.5)
        query_pos = offset + begin + jnp.arange(BLOCK, dtype=jnp.int32)
        key_pos = offset + begin - WINDOW + jnp.arange(span, dtype=jnp.int32)
        allowed = (
            (jnp.abs(query_pos[:, None] - key_pos[None, :]) <= WINDOW)
            & (key_pos >= 0)[None, :]
            & (key_pos < total)[None, :]
        )
        scores = jnp.where(allowed, scores, NEG_FILL)
        top = jnp.maximum(jnp.max(scores, axis=-1), sink_group)
        expo = jnp.exp(scores - top[..., None])
        denom = jnp.sum(expo, axis=-1) + jnp.exp(sink_group - top)
        weights = (expo / denom[..., None]).astype(jnp.bfloat16)
        return jnp.einsum(
            "kgqn,nkd->qkgd", weights, value_block, preferred_element_type=jnp.float32
        ).astype(jnp.bfloat16)

    result = lax.map(one_block, (jnp.arange(nblocks, dtype=jnp.int32), shaped))
    return result.reshape(count, local_heads * HEAD_DIM)


def per_device(
    tokens,
    norm_gain,
    query_weight,
    key_weight,
    value_weight,
    gate_weight,
    left_weight,
    input_weight,
    query_gain,
    key_gain,
    sink_logit,
    conv_weight,
    out_attention,
    out_conv,
):
    sp_count = lax.axis_size("sp")
    sp_place = lax.axis_index("sp")
    gathered = (
        lax.all_gather(query_weight, "sp", axis=1, tiled=True),
        lax.all_gather(key_weight, "sp", axis=1, tiled=True),
        lax.all_gather(value_weight, "sp", axis=1, tiled=True),
        lax.all_gather(gate_weight, "sp", axis=1, tiled=True),
        lax.all_gather(left_weight, "sp", axis=1, tiled=True),
        lax.all_gather(input_weight, "sp", axis=1, tiled=True),
        lax.all_gather(out_attention, "sp", axis=1, tiled=True),
        lax.all_gather(out_conv, "sp", axis=1, tiled=True),
    )
    (
        query_full,
        key_full,
        value_full,
        gate_full,
        left_full,
        input_full,
        attn_out_full,
        conv_out_full,
    ) = gathered
    normed = normalize(tokens.astype(jnp.float32), norm_gain).astype(jnp.bfloat16)
    widths = [
        query_full.shape[0],
        key_full.shape[0],
        value_full.shape[0],
        gate_full.shape[0],
        left_full.shape[0],
        input_full.shape[0],
    ]
    piece = lax.all_gather(normed, "tp", axis=0, tiled=True)
    joined = jnp.concatenate(
        [
            project(piece, weight)
            for weight in (query_full, key_full, value_full, gate_full, left_full, input_full)
        ],
        axis=1,
    )
    count = joined.shape[0]
    bounds = [0]
    for width in widths:
        bounds.append(bounds[-1] + width)
    query, keys, values, gate, left, inputs = [
        joined[:, bounds[place] : bounds[place + 1]] for place in range(6)
    ]
    offset = sp_place * count
    total = count * sp_count
    positions = (offset + jnp.arange(count, dtype=jnp.int32)).astype(jnp.float32)
    local_heads = widths[0] // HEAD_DIM
    kv_local = widths[1] // HEAD_DIM
    query_rot = rotate(
        normalize(query.reshape(count, local_heads, HEAD_DIM).astype(jnp.float32), query_gain),
        positions,
    ).astype(jnp.bfloat16)
    key_rot = rotate(
        normalize(keys.reshape(count, kv_local, HEAD_DIM).astype(jnp.float32), key_gain), positions
    ).astype(jnp.bfloat16)
    key_flat = key_rot.reshape(count, kv_local * HEAD_DIM)
    product = (left.astype(jnp.float32) * inputs.astype(jnp.float32)).astype(jnp.bfloat16)
    kv_width = widths[1]
    pair_rim = with_halo(jnp.concatenate([key_flat, values], axis=1), (("sp", 0),), WINDOW)
    product_rim = with_halo(product, (("sp", 0),), 1)
    rim_rows = pair_rim.shape[0]
    key_rim = pair_rim[:, :kv_width].reshape(rim_rows, kv_local, HEAD_DIM)
    value_rim = pair_rim[:, kv_width:].reshape(rim_rows, kv_local, HEAD_DIM)
    attended = attend(query_rot, key_rim, value_rim, sink_logit, offset, total)
    padded = product_rim.astype(jnp.float32)
    convolved = (
        conv_weight[0] * padded[:-2] + conv_weight[1] * padded[1:-1] + conv_weight[2] * padded[2:]
    )
    gated = (gate.astype(jnp.float32) * convolved).astype(jnp.bfloat16)
    return lax.psum_scatter(
        (
            jnp.dot(attended, attn_out_full, preferred_element_type=jnp.float32)
            + jnp.dot(gated, conv_out_full, preferred_element_type=jnp.float32)
        ).astype(jnp.bfloat16),
        "tp",
        scatter_dimension=0,
        tiled=True,
    )


MESH = pl.DeviceIdType.MESH


def fused_kernel(
    dims,
    tok_hbm, gain_ref, q_hbm, k_hbm, v_hbm, g_hbm, l_hbm, i_hbm,
    qgain_ref, kgain_ref, sink_ref, conv_ref, oa_hbm, oc_hbm, trig_hbm,
    out_ref,
    tok, trig, stage, ostage, win, wout, normed, normed2, acc, acc2, rim, prod, prod2, mix_a, mix_c, gated2,
    qrot,
    keep, s1, r1, s2, r2, s3, r3,
    local_sem, y_send, oy_send, in_recv, out_recv, in_up, in_down, out_up, out_down,
    tok_send, tok_recv, tok2_send, tok2_recv, rim_send, rim_recv, prod_send, prod_recv, g_send, g_recv,
    rs_send, rs_recv,
):
    line, rows, depth, qr, kr, cr = (
        dims["line"], dims["rows"], dims["depth"], dims["qr"], dims["kr"], dims["cr"]
    )
    sp = lax.axis_index("sp")
    tp = lax.axis_index("tp")
    z, y = sp // 2, sp % 2
    x, c = tp // 2, tp % 2
    y_peer = (2 * z + 1 - y, tp)
    x_peer = (sp, 2 * (1 - x) + c)
    c_peer = (sp, 2 * x + 1 - c)
    up = (jnp.minimum(2 * (z + 1) + y, 2 * line - 1), tp)
    down = (jnp.maximum(2 * (z - 1) + y, 0), tp)
    has_up = z < line - 1
    has_down = z > 0
    s_own = sp
    s_mate = 2 * z + 1 - y
    plane = 8 * rows
    core = qr + 2 * kr
    is_end = (z == 0) | (z == line - 1)
    not_end = (z > 0) & (z < line - 1)
    is_help = (z == 1) | (z == line - 2)
    help_dev = (jnp.where(z == 0, 2 + y, 2 * (line - 2) + y), tp)
    end_dev = (jnp.where(z == 1, y, 2 * (line - 1) + y), tp)

    barrier = pltpu.get_barrier_semaphore()
    for peer in (y_peer, x_peer, c_peer):
        pl.semaphore_signal(barrier, inc=1, device_id=peer, device_id_type=MESH)

    @pl.when(has_up)
    def _():
        pl.semaphore_signal(barrier, inc=1, device_id=up, device_id_type=MESH)

    @pl.when(has_down)
    def _():
        pl.semaphore_signal(barrier, inc=1, device_id=down, device_id_type=MESH)

    counter = [0]

    def local(src, dst):
        copy = pltpu.make_async_copy(src, dst, local_sem.at[counter[0]])
        counter[0] += 1
        copy.start()
        return copy

    def pieces(which, dst):
        q0, c0 = pl.multiple_of(which * qr, qr), pl.multiple_of(which * cr, cr)
        return [
            local(q_hbm.at[pl.ds(q0, qr)], dst.at[0:qr]),
            local(k_hbm, dst.at[qr : qr + kr]),
            local(v_hbm, dst.at[qr + kr : qr + 2 * kr]),
            local(g_hbm.at[pl.ds(c0, cr)], dst.at[qr + 2 * kr : qr + 2 * kr + cr]),
            local(l_hbm.at[pl.ds(c0, cr)], dst.at[qr + 2 * kr + cr : qr + 2 * kr + 2 * cr]),
            local(i_hbm.at[pl.ds(c0, cr)], dst.at[qr + 2 * kr + 2 * cr : qr + 2 * kr + 3 * cr]),
        ]

    def out_pieces(which, dst):
        q0, c0 = pl.multiple_of(which * qr, qr), pl.multiple_of(which * cr, cr)
        return [
            local(oa_hbm.at[pl.ds(q0, qr)], dst.at[0:qr]),
            local(oc_hbm.at[pl.ds(c0, cr)], dst.at[qr : qr + cr]),
        ]

    mine = pieces(y, win.at[s_own])
    theirs = pieces(1 - y, stage)
    tok_copy = local(tok_hbm, tok)
    out_theirs = out_pieces(1 - y, ostage)
    out_mine = out_pieces(y, wout.at[s_own])
    trig_copy = local(trig_hbm.at[pl.ds(pl.multiple_of(z * plane, plane), plane)], trig)

    pl.semaphore_wait(barrier, 3 + has_up.astype(jnp.int32) + has_down.astype(jnp.int32))

    def remote(src, dst, send, recv, peer):
        return pltpu.make_async_remote_copy(
            src_ref=src, dst_ref=dst, send_sem=send, recv_sem=recv,
            device_id=peer, device_id_type=MESH,
        )

    def hop(buf, s, send, recv, peer):
        return remote(buf.at[s], buf.at[s], send.at[s], recv.at[s], peer)

    chunks = ((0, core), (core, core + 3 * cr))

    def in_hop(s, part, send, peer):
        lo, hi = chunks[part]
        return remote(
            win.at[s, lo:hi], win.at[s, lo:hi], send.at[part, s], in_recv.at[part, s], peer
        )

    def in_sends(s, source, part, act):
        for inner, edge, way, send, peer in (
            (z + 1 < line - 1, has_up, source <= z, in_up, up),
            (z - 1 > 0, has_down, source >= z, in_down, down),
        ):
            @pl.when(way & (edge if part == 0 else inner))
            def _():
                act(in_hop(s, part, send, peer))

    def in_forward(s, source, part):
        in_sends(s, source, part, lambda copy: copy.start())

    up_full = z + 1 < line - 1
    down_full = z - 1 > 0

    def forward(buf, s, source, ups, downs, recv):
        @pl.when((source <= z) & has_up)
        def _():
            hop(buf, s, ups, recv, up).start()

        @pl.when((source >= z) & has_down)
        def _():
            hop(buf, s, downs, recv, down).start()

    for copy in mine:
        copy.wait()
    for part in range(2):
        in_forward(s_own, z, part)
    for copy in theirs:
        copy.wait()
    y_copies = [
        remote(
            stage.at[lo:hi], win.at[s_own, lo:hi], y_send.at[part], in_recv.at[part, s_own], y_peer
        )
        for part, (lo, hi) in enumerate(chunks)
    ]
    for copy in y_copies:
        copy.start()
    tok_copy.wait()
    t = tok[...].astype(jnp.float32)
    t = t * lax.rsqrt(jnp.mean(t * t, axis=-1, keepdims=True) + EPS) * gain_ref[...]
    own_block = 4 * y + 2 * x + c
    normed[own_block] = t.astype(jnp.bfloat16)

    def end_tok(block, slot):
        return remote(
            normed.at[block], normed2.at[block], tok2_send.at[slot], tok2_recv.at[block], help_dev
        )

    def tok2_hop(block, slot, peer):
        return remote(
            normed2.at[block], normed2.at[block], tok2_send.at[slot], tok2_recv.at[block], peer
        )

    for copy in out_theirs:
        copy.wait()
    oy_copy = remote(ostage, wout.at[s_own], oy_send.at[0], out_recv.at[s_own], y_peer)
    oy_copy.start()
    for copy in out_mine:
        copy.wait()

    @pl.when(is_end)
    def _():
        end_tok(own_block, 0).start()

    def block_of(yy, xx, cc):
        return 4 * yy + 2 * xx + cc

    def tok_hop(block, slot, peer):
        return remote(
            normed.at[block], normed.at[block], tok_send.at[slot], tok_recv.at[block], peer
        )

    xb = block_of(y, 1 - x, c)
    yb0 = block_of(1 - y, x, c)
    yb1 = block_of(1 - y, 1 - x, c)
    tok_copies = [
        tok_hop(own_block, 0, x_peer),
        tok_hop(own_block, 1, y_peer),
        tok_hop(own_block, 2, c_peer),
    ]
    for copy in tok_copies:
        copy.start()

    for part in range(2):
        in_hop(s_mate, part, in_up, up).wait_recv()
        in_forward(s_mate, z, part)

    def tok_wait(block):
        tok_hop(block, 0, x_peer).wait_recv()

    tok_wait(xb)
    more = [tok_hop(xb, 3, y_peer), tok_hop(xb, 4, c_peer)]
    for copy in more:
        copy.start()
    tok_copies += more

    hop(wout, s_mate, out_up, out_recv, up).wait_recv()

    def own_out(flag_up, flag_down):
        for s in (s_own, s_mate):
            @pl.when(flag_up & has_up)
            def _():
                hop(wout, s, out_up, out_recv, up).start()

            @pl.when(flag_down & has_down)
            def _():
                hop(wout, s, out_down, out_recv, down).start()

    tok_wait(yb0)

    @pl.when(is_end)
    def _():
        end_tok(yb0, 1).start()

    own_out(z == 0, z == line - 1)
    copy = tok_hop(yb0, 5, c_peer)
    copy.start()
    tok_copies.append(copy)
    tok_wait(yb1)
    copy = tok_hop(yb1, 6, c_peer)
    copy.start()
    tok_copies.append(copy)
    for yy in range(2):
        for xx in range(2):
            tok_wait(block_of(yy, xx, 1 - c))

    def columns(s):
        return pl.ds(pl.multiple_of(s * depth, depth), depth)

    def dot_t(a, w):
        return lax.dot_general(a, w, (((1,), (1,)), ((), ())), preferred_element_type=jnp.float32)

    def in_dot(s, first):
        a = normed[:, :, columns(s)].reshape(plane, depth)
        low_part = dot_t(a, win[s, 0:core])
        acc[:, 0:core] = low_part if first else acc[:, 0:core] + low_part

        @pl.when(not_end)
        def _():
            high_part = dot_t(a, win[s, core:])
            acc[:, core:] = high_part if first else acc[:, core:] + high_part

    paired = jnp.minimum(z, line - 1 - z)
    below_longer = z > line - 1 - z

    def source_of(k):
        d = jnp.where(k <= 2 * paired, (k + 1) // 2, k - paired)
        below = jnp.where(k <= 2 * paired, k % 2 == 1, below_longer)
        return jnp.where(below, z - d, z + d)

    in_dot(s_own, True)
    in_dot(s_mate, False)

    def in_step(k, carry):
        source = source_of(k)
        for turn, block, slot in ((2, own_block, 2), (line - 1, yb0, 4)):
            @pl.when(is_help & (k == turn))
            def _():
                tok2_hop(block, slot, end_dev).wait_recv()
                tok2_hop(block, slot, x_peer).start()
                tok2_hop(block, slot + 1, c_peer).start()

        for half in range(2):
            first = jnp.where(half == 0, y, 1 - y)
            s = 2 * source + first
            in_hop(s, 0, in_up, up).wait_recv()
            in_forward(s, source, 0)

            @pl.when(not_end)
            def _():
                in_hop(s, 1, in_up, up).wait_recv()
                in_forward(s, source, 1)

            if half == 1:
                own_out(source == 0, source == line - 1)
            in_dot(s, False)
        return carry

    lax.fori_loop(1, line, in_step, 0)

    trig_copy.wait()
    lane = lax.broadcasted_iota(jnp.int32, (plane, qr), 1)
    half_dim = HEAD_DIM // 2
    table = trig[...]
    cos2 = jnp.where(lane < HEAD_DIM, table, pltpu.roll(table, HEAD_DIM, 1))
    sin2 = jnp.where(lane < HEAD_DIM, pltpu.roll(table, HEAD_DIM, 1), table)
    low = lane < HEAD_DIM
    first_half = lane % HEAD_DIM < half_dim

    def rot(v):
        partner = jnp.where(
            first_half, pltpu.roll(v, qr - half_dim, 1), pltpu.roll(v, half_dim, 1)
        )
        return v * cos2 + partner * sin2

    def bf(v):
        return v.astype(jnp.bfloat16).astype(jnp.float32)

    kv = bf(acc[:, qr : 2 * qr])
    ksq = jnp.sum(jnp.where(low, kv * kv, 0.0), axis=-1, keepdims=True) / HEAD_DIM
    kgain = jnp.concatenate([kgain_ref[...], kgain_ref[...]], axis=1)
    kn = kv * lax.rsqrt(ksq + EPS) * kgain
    krot = rot(kn)
    rim[WINDOW : WINDOW + plane, :] = jnp.where(low, krot, kv).astype(jnp.bfloat16)
    base = 2 * qr

    qv = bf(acc[:, 0:qr])
    qq = qv * qv
    q_lo = jnp.sum(jnp.where(low, qq, 0.0), axis=-1, keepdims=True) / HEAD_DIM
    q_hi = jnp.sum(jnp.where(low, 0.0, qq), axis=-1, keepdims=True) / HEAD_DIM
    qgain = jnp.concatenate([qgain_ref[...], qgain_ref[...]], axis=1)
    qn = qv * lax.rsqrt(jnp.where(low, q_lo, q_hi) + EPS) * qgain
    qro = rot(qn)

    bottom = pl.ds(WINDOW, WINDOW)
    top = pl.ds(plane, WINDOW)
    rim_up = remote(rim.at[top], rim.at[pl.ds(0, WINDOW)], rim_send.at[0], rim_recv.at[0], up)
    rim_down = remote(
        rim.at[bottom], rim.at[pl.ds(WINDOW + plane, WINDOW)], rim_send.at[1], rim_recv.at[1], down
    )

    @pl.when(has_up)
    def _():
        rim_up.start()

    @pl.when(has_down)
    def _():
        rim_down.start()

    zero_rim = jnp.zeros((WINDOW, qr), jnp.bfloat16)

    @pl.when(z == 0)
    def _():
        rim[0:WINDOW] = zero_rim

    @pl.when(z == line - 1)
    def _():
        rim[WINDOW + plane :] = zero_rim

    qrot[0] = jnp.where(low, qro, 0.0).astype(jnp.bfloat16)
    qrot[1] = jnp.where(low, pltpu.roll(qro, HEAD_DIM, 1), 0.0).astype(jnp.bfloat16)

    pad = 16
    zero_pad = jnp.zeros((pad, cr), jnp.bfloat16)
    taps = conv_ref[y]

    def convolve(ref, gate):
        p = ref[...].astype(jnp.float32)
        before = pltpu.roll(p, 1, 0)[pad : pad + plane]
        after = pltpu.roll(p, plane + 2 * pad - 1, 0)[pad : pad + plane]
        mixed = taps[0:1] * before + taps[1:2] * p[pad : pad + plane] + taps[2:3] * after
        return (gate * mixed).astype(jnp.bfloat16)

    prod_up = remote(
        prod.at[pl.ds(plane, pad)], prod.at[pl.ds(0, pad)], prod_send.at[0], prod_recv.at[0], up
    )
    prod_down = remote(
        prod.at[pl.ds(pad, pad)], prod.at[pl.ds(pad + plane, pad)],
        prod_send.at[1], prod_recv.at[1], down,
    )
    from_up = not_end & up_full
    from_down = not_end & down_full

    @pl.when(not_end)
    def _():
        left = bf(acc[:, base + cr : base + 2 * cr])
        inputs = bf(acc[:, base + 2 * cr : base + 3 * cr])
        prod[pad : pad + plane] = (left * inputs).astype(jnp.bfloat16)

    @pl.when(from_up)
    def _():
        prod_up.start()

    @pl.when(from_down)
    def _():
        prod_down.start()

    def out_take(k):
        source = source_of(jnp.int32(k))
        for half in range(2):
            s = 2 * source + half
            hop(wout, s, out_up, out_recv, up).wait_recv()
            forward(wout, s, source, out_up, out_down, out_recv)

    def inner_take(k):
        @pl.when(not_end)
        def _():
            out_take(k)

    inner_take(1)
    g_copy = remote(gated2, mix_c, g_send.at[0], g_recv.at[0], end_dev)

    @pl.when(is_help)
    def _():
        for block, slot in ((xb, 6), (yb1, 7)):
            tok2_hop(block, slot, x_peer).wait_recv()
            tok2_hop(block, slot, c_peer).start()
        for yy in range(2):
            for xx in range(2):
                tok2_hop(block_of(yy, xx, 1 - c), 0, c_peer).wait_recv()
        acc2[...] = jnp.zeros_like(acc2)

        def help_step(s, carry):
            a = normed2[:, :, columns(s)].reshape(plane, depth)
            acc2[...] += dot_t(a, win[s, core:])
            return carry

        lax.fori_loop(0, 2 * line, help_step, 0)
        prod2[pad : pad + plane] = (
            bf(acc2[:, cr : 2 * cr]) * bf(acc2[:, 2 * cr : 3 * cr])
        ).astype(jnp.bfloat16)

        @pl.when(z == 1)
        def _():
            prod2[0:pad] = zero_pad
            prod2[pad + plane :] = prod[pad : 2 * pad]
            prod[0:pad] = prod2[plane : plane + pad]

        @pl.when(z != 1)
        def _():
            prod2[0:pad] = prod[plane : plane + pad]
            prod2[pad + plane :] = zero_pad
            prod[pad + plane :] = prod2[pad : 2 * pad]

        gated2[...] = convolve(prod2, bf(acc2[:, 0:cr]))
        g_copy.start()

    @pl.when(from_up)
    def _():
        prod_down.wait_recv()

    @pl.when(from_down)
    def _():
        prod_up.wait_recv()

    @pl.when(not_end)
    def _():
        mix_c[...] = convolve(prod, bf(acc[:, base : base + cr]))

    for k in range(2, line - 1):
        inner_take(k)

    @pl.when(has_down)
    def _():
        rim_up.wait_recv()

    @pl.when(has_up)
    def _():
        rim_down.wait_recv()

    span = BLOCK + 2 * WINDOW
    total = plane * line

    def att_step(block, carry):
        begin = pl.multiple_of(block * BLOCK, BLOCK)
        kvb = rim[pl.ds(begin, span), :]
        qb = qrot[:, pl.ds(begin, BLOCK), :].reshape(2 * BLOCK, qr)
        scores = lax.dot_general(
            qb, kvb, (((1,), (1,)), ((), ())), preferred_element_type=jnp.float32
        ) * HEAD_DIM ** (-0.5)
        row = lax.broadcasted_iota(jnp.int32, (2 * BLOCK, span), 0)
        col = lax.broadcasted_iota(jnp.int32, (2 * BLOCK, span), 1)
        gap = row % BLOCK + WINDOW - col
        pos = z * plane + begin - WINDOW + col
        allowed = (gap <= WINDOW) & (gap >= -WINDOW) & (pos >= 0) & (pos < total)
        scores = jnp.where(allowed, scores, NEG_FILL)
        head = lax.broadcasted_iota(jnp.int32, (2 * BLOCK, 1), 0)
        sink = jnp.where(head < BLOCK, sink_ref[0, 2 * y], sink_ref[0, 2 * y + 1])
        peak = jnp.maximum(jnp.max(scores, axis=-1, keepdims=True), sink)
        expo = jnp.exp(scores - peak)
        denom = jnp.sum(expo, axis=-1, keepdims=True) + jnp.exp(sink - peak)
        weights = (expo / denom).astype(jnp.bfloat16)
        o = jnp.dot(weights, kvb, preferred_element_type=jnp.float32)
        low_b = lax.broadcasted_iota(jnp.int32, (BLOCK, qr), 1) < HEAD_DIM
        both = jnp.where(low_b, pltpu.roll(o[:BLOCK], HEAD_DIM, 1), o[BLOCK:])
        mix_a[pl.ds(begin, BLOCK), :] = both.astype(jnp.bfloat16)
        return carry

    lax.fori_loop(0, plane // BLOCK, att_step, 0)

    @pl.when(is_end)
    def _():
        g_copy.wait_recv()

    def group(cc):
        spans = [pl.ds(pl.multiple_of((2 * q + cc) * rows, rows), rows) for q in range(4)]
        return [jnp.concatenate([mix_a[w, :], mix_c[w, :]], axis=1) for w in spans]

    mine_rows = jnp.concatenate(group(c), axis=0)
    other_rows = jnp.concatenate(group(1 - c), axis=0)
    rs_copies = []

    def send_rs(src, dst, stage_id, s, peer):
        copy = remote(src, dst, rs_send.at[stage_id, s], rs_recv.at[stage_id, s], peer)
        copy.start()
        rs_copies.append(copy)

    def stage_a(k):
        source = z if k == 0 else source_of(jnp.int32(k))
        if k:
            @pl.when(is_end)
            def _():
                out_take(k)

        for half in range(2):
            s = 2 * source + half
            weight = wout[s]
            s1[s] = jnp.dot(
                other_rows, weight, preferred_element_type=jnp.float32
            ).astype(jnp.bfloat16).reshape(2, 2, rows, depth)
            send_rs(s1.at[s], r1.at[s], 0, s, c_peer)
            keep[s] = jnp.dot(
                mine_rows, weight, preferred_element_type=jnp.float32
            ).reshape(2, 2, rows, depth)

    def axis_index_of(half):
        return (y, x) if half == 0 else (x, y)

    def stage_b(k):
        source = z if k == 0 else source_of(jnp.int32(k))
        for half in range(2):
            s = 2 * source + half
            remote(s1.at[s], r1.at[s], rs_send.at[0, s], rs_recv.at[0, s], c_peer).wait_recv()
            for j in range(2):
                if half == 0:
                    s2[s, j] = (keep[s, 1 - y, j] + r1[s, 1 - y, j].astype(jnp.float32)).astype(
                        jnp.bfloat16
                    )
                else:
                    s2[s, j] = (keep[s, j, 1 - x] + r1[s, j, 1 - x].astype(jnp.float32)).astype(
                        jnp.bfloat16
                    )
            send_rs(s2.at[s], r2.at[s], 1, s, y_peer if half == 0 else x_peer)

    def stage_c(k):
        source = z if k == 0 else source_of(jnp.int32(k))
        for half in range(2):
            s = 2 * source + half
            peer = y_peer if half == 0 else x_peer
            remote(s2.at[s], r2.at[s], rs_send.at[1, s], rs_recv.at[1, s], peer).wait_recv()
            my = x if half == 0 else y
            for own, j in ((False, 1 - my), (True, my)):
                if half == 0:
                    part = keep[s, y, j] + r1[s, y, j].astype(jnp.float32)
                else:
                    part = keep[s, j, x] + r1[s, j, x].astype(jnp.float32)
                part = part + r2[s, j].astype(jnp.float32)
                if own:
                    keep[s, y, x] = part
                else:
                    s3[s] = part.astype(jnp.bfloat16)
                    send_rs(s3.at[s], r3.at[s], 2, s, x_peer if half == 0 else y_peer)

    def stage_d(k):
        source = z if k == 0 else source_of(jnp.int32(k))
        for half in range(2):
            s = 2 * source + half
            peer = x_peer if half == 0 else y_peer
            remote(s3.at[s], r3.at[s], rs_send.at[2, s], rs_recv.at[2, s], peer).wait_recv()
            out_ref[:, columns(s)] = (keep[s, y, x] + r3[s].astype(jnp.float32)).astype(
                jnp.bfloat16
            )

    for k in range(line + 3):
        if k == line - 1:
            inner_take(k)
        for late, step in enumerate((stage_a, stage_b, stage_c, stage_d)):
            if 0 <= k - late < line:
                step(k - late)

    for copy in y_copies + [oy_copy] + tok_copies + rs_copies:
        copy.wait_send()

    @pl.when(has_up)
    def _():
        rim_up.wait_send()

    @pl.when(has_down)
    def _():
        rim_down.wait_send()

    @pl.when(is_end)
    def _():
        end_tok(own_block, 0).wait_send()
        end_tok(yb0, 1).wait_send()

    @pl.when(is_help)
    def _():
        for slot in range(2, 8):
            tok2_hop(own_block, slot, x_peer).wait_send()
        g_copy.wait_send()

    @pl.when(from_up)
    def _():
        prod_up.wait_send()

    @pl.when(from_down)
    def _():
        prod_down.wait_send()

    for s in range(2 * line):
        for part in range(2):
            in_sends(s, s // 2, part, lambda copy: copy.wait_send())

        @pl.when((s // 2 <= z) & has_up)
        def _():
            hop(wout, s, out_up, out_recv, up).wait_send()

        @pl.when((s // 2 >= z) & has_down)
        def _():
            hop(wout, s, out_down, out_recv, down).wait_send()


def trig_table(total):
    half = HEAD_DIM // 2
    freq = np.float64(ROPE_BASE) ** (-np.arange(half) / half)
    angle = np.arange(total)[:, None] * freq
    cosine, sine = np.cos(angle), np.sin(angle)
    return np.concatenate([cosine, cosine, -sine, sine], axis=1).astype(np.float32)


def fused_device(
    tokens, norm_gain, query_weight, key_weight, value_weight, gate_weight, left_weight,
    input_weight, query_gain, key_gain, sink_logit, conv_weight, out_attention, out_conv,
):
    sp_count = lax.axis_size("sp")
    line = sp_count // 2
    rows, width = tokens.shape
    depth = query_weight.shape[1]
    qr = query_weight.shape[0] // 2
    kr = key_weight.shape[0]
    cr = gate_weight.shape[0] // 2
    fan = qr + 2 * kr + 3 * cr
    plane = 8 * rows
    dims = dict(line=line, rows=rows, depth=depth, qr=qr, kr=kr, cr=cr)
    vm = pl.BlockSpec(memory_space=pltpu.VMEM)
    sm = pl.BlockSpec(memory_space=pltpu.SMEM)
    hb = pl.BlockSpec(memory_space=pl.ANY)
    bf16, f32 = jnp.bfloat16, jnp.float32
    dma = pltpu.SemaphoreType.DMA
    n = sp_count
    scratch = [
        pltpu.VMEM((rows, width), bf16),
        pltpu.VMEM((plane, 2 * HEAD_DIM), f32),
        pltpu.VMEM((fan, depth), bf16),
        pltpu.VMEM((qr + cr, depth), bf16),
        pltpu.VMEM((n, fan, depth), bf16),
        pltpu.VMEM((n, qr + cr, depth), bf16),
        pltpu.VMEM((8, rows, width), bf16),
        pltpu.VMEM((8, rows, width), bf16),
        pltpu.VMEM((plane, fan), f32),
        pltpu.VMEM((plane, 3 * cr), f32),
        pltpu.VMEM((plane + 2 * WINDOW, qr), bf16),
        pltpu.VMEM((plane + 32, cr), bf16),
        pltpu.VMEM((plane + 32, cr), bf16),
        pltpu.VMEM((plane, qr), bf16),
        pltpu.VMEM((plane, cr), bf16),
        pltpu.VMEM((plane, cr), bf16),
        pltpu.VMEM((2, plane, qr), bf16),
        pltpu.VMEM((n, 2, 2, rows, depth), f32),
        pltpu.VMEM((n, 2, 2, rows, depth), bf16),
        pltpu.VMEM((n, 2, 2, rows, depth), bf16),
        pltpu.VMEM((n, 2, rows, depth), bf16),
        pltpu.VMEM((n, 2, rows, depth), bf16),
        pltpu.VMEM((n, rows, depth), bf16),
        pltpu.VMEM((n, rows, depth), bf16),
        dma((18,)), dma((2,)), dma((1,)), dma((2, n)), dma((n,)),
        dma((2, n)), dma((2, n)), dma((n,)), dma((n,)),
        dma((7,)), dma((8,)), dma((8,)), dma((8,)), dma((2,)), dma((2,)), dma((2,)), dma((2,)),
        dma((1,)), dma((1,)), dma((3, n)), dma((3, n)),
    ]
    taps = conv_weight.reshape(3, 2, cr).transpose(1, 0, 2)
    return pl.pallas_call(
        functools.partial(fused_kernel, dims),
        out_shape=jax.ShapeDtypeStruct((rows, width), bf16),
        in_specs=[hb, vm, hb, hb, hb, hb, hb, hb, vm, vm, sm, vm, hb, hb, hb],
        out_specs=vm,
        scratch_shapes=scratch,
        compiler_params=pltpu.CompilerParams(
            collective_id=0, has_side_effects=True, vmem_limit_bytes=56 * 1024 * 1024
        ),
    )(
        tokens, norm_gain[None, :], query_weight, key_weight, value_weight, gate_weight,
        left_weight, input_weight, query_gain[None, :],
        key_gain[None, :], sink_logit[None, :], taps, out_attention, out_conv,
        jnp.asarray(trig_table(plane * line)),
    )


def local_device(*args):
    tokens, query_weight, key_weight, gate_weight = args[0], args[2], args[3], args[5]
    fits = (
        lax.axis_size("sp") % 2 == 0
        and 8 <= lax.axis_size("sp") <= 16
        and lax.axis_size("tp") == 4
        and query_weight.shape[1] % 128 == 0
        and query_weight.shape[0] == 4 * HEAD_DIM
        and key_weight.shape[0] == HEAD_DIM
        and gate_weight.shape[0] == 256
        and tokens.shape[0] % 16 == 0
        and 8 * tokens.shape[0] % BLOCK == 0
    )
    return fused_device(*args) if fits else per_device(*args)


def solution(mesh):
    in_specs = (
        P(("sp", "tp"), None),
        P(),
        P("tp", "sp"),
        P("tp", "sp"),
        P("tp", "sp"),
        P("tp", "sp"),
        P("tp", "sp"),
        P("tp", "sp"),
        P(),
        P(),
        P("tp"),
        P(None, "tp"),
        P("tp", "sp"),
        P("tp", "sp"),
    )
    out_specs = P(("sp", "tp"), None)
    return jax.shard_map(
        local_device, mesh=mesh, in_specs=in_specs, out_specs=out_specs, check_vma=False
    )
```

profile of v0, /device:TPU:0, one launch (start us, length us, event | category | flops | bytes accessed | tf_op | source)
XLA Modules:
  0.0 82.6 jit_solution(4938804896205299164)
XLA Ops:
  0.0 80.9 %shard_map.145 = bf16[64,2048]{1,0:T(8,128)(2,1)} custom-call(bf16[64,2048]{1,0:T(8,128)(2,1)} %tok_hbm.1, f32[1,2048]{1,0:T(1,128)} %bitcast.7, bf16[256,256]{1,0:T(8,128)(2,1)} %q_hbm.1, bf16[64,256]{1,0:T(8,128)(2,1)} %k_hbm.1, bf16[64,256]{1,0:T(8,128)(2,1)} %v_hbm.1, bf16[256,256]{1,0:T(8,128)(2,1)} %g_hbm.1, bf16[256,256]{1,0:T(8,128)(2,1)} %l_hbm.1, ...), custom_call_target="tpu_custom_call" | custom-call | tf_op jit(solution)/shard_map/pallas_call | solution.py:874
  80.9 1.7 %copy.17 = bf16[64,2048]{1,0:T(8,128)(2,1)} copy(bf16[64,2048]{1,0:T(8,128)(2,1)} %shard_map.145) | data formatting | bytes 524288
where the time goes:
time: 82.8 us; the launch traced here: 82.6 us
  Pallas kernels  80.9 us (98%)
  local copies, waits for them, and re-layouts  1.67 us (2%)
    pallas_call x1, Pallas kernels, fused_device(): pl.pallas_call(functools.partial(fused_kernel, dims), out_shape=jax.Shape...  80.9 us
    unnamed x1, local copies, waits for them, and re-layouts  1.67 us

commit v1 on v0

v1 whole, which is shorter than its diff:
```python
import functools

import jax
import jax.numpy as jnp
import numpy as np
from jax import lax
from jax.experimental import pallas as pl
from jax.experimental.pallas import tpu as pltpu
from jax.sharding import PartitionSpec as P

HEAD_DIM = 64
WINDOW = 128
BLOCK = 128


EPS = 1e-06
ROPE_BASE = 10000.0
NEG_FILL = -1e30


def with_halo(cells, sides, width):
    for axis, dim in sides:
        count = lax.axis_size(axis)
        ends = count - 1
        head = lax.slice_in_dim(cells, 0, width, axis=dim)
        tail = lax.slice_in_dim(cells, cells.shape[dim] - width, cells.shape[dim], axis=dim)
        cells = jnp.concatenate(
            [
                lax.ppermute(tail, axis, [(i, (i + 1) % count) for i in range(ends)]),
                cells,
                lax.ppermute(head, axis, [((i + 1) % count, i) for i in range(ends)]),
            ],
            axis=dim,
        )
    return cells


def normalize(values, gain):
    return values * lax.rsqrt(jnp.mean(values * values, axis=-1, keepdims=True) + EPS) * gain


def rotate(values, positions):
    half = values.shape[-1] // 2
    freq = ROPE_BASE ** (-jnp.arange(half, dtype=jnp.float32) / half)
    angle = positions[:, None] * freq
    cosine = jnp.cos(angle)[:, None, :]
    sine = jnp.sin(angle)[:, None, :]
    first = values[..., :half]
    second = values[..., half:]
    return jnp.concatenate(
        [first * cosine - second * sine, second * cosine + first * sine], axis=-1
    )


def project(rows, weight):
    return lax.dot_general(
        rows, weight, (((1,), (1,)), ((), ())), preferred_element_type=jnp.float32
    ).astype(jnp.bfloat16)


def attend(query_rot, key_rim, value_rim, sinks, offset, total):
    count = query_rot.shape[0]
    local_heads = query_rot.shape[1]
    kv_local = key_rim.shape[1]
    group = local_heads // kv_local
    span = BLOCK + 2 * WINDOW
    nblocks = count // BLOCK
    shaped = query_rot.reshape(nblocks, BLOCK, kv_local, group, HEAD_DIM)
    sink_group = sinks.reshape(kv_local, group)[:, :, None]

    def one_block(packed):
        block_index, query_block = packed
        begin = block_index * BLOCK
        key_block = lax.dynamic_slice_in_dim(key_rim, begin, span, 0)
        value_block = lax.dynamic_slice_in_dim(value_rim, begin, span, 0)
        scores = jnp.einsum(
            "qkgd,nkd->kgqn", query_block, key_block, preferred_element_type=jnp.float32
        ) * HEAD_DIM ** (-0.5)
        query_pos = offset + begin + jnp.arange(BLOCK, dtype=jnp.int32)
        key_pos = offset + begin - WINDOW + jnp.arange(span, dtype=jnp.int32)
        allowed = (
            (jnp.abs(query_pos[:, None] - key_pos[None, :]) <= WINDOW)
            & (key_pos >= 0)[None, :]
            & (key_pos < total)[None, :]
        )
        scores = jnp.where(allowed, scores, NEG_FILL)
        top = jnp.maximum(jnp.max(scores, axis=-1), sink_group)
        expo = jnp.exp(scores - top[..., None])
        denom = jnp.sum(expo, axis=-1) + jnp.exp(sink_group - top)
        weights = (expo / denom[..., None]).astype(jnp.bfloat16)
        return jnp.einsum(
            "kgqn,nkd->qkgd", weights, value_block, preferred_element_type=jnp.float32
        ).astype(jnp.bfloat16)

    result = lax.map(one_block, (jnp.arange(nblocks, dtype=jnp.int32), shaped))
    return result.reshape(count, local_heads * HEAD_DIM)


def per_device(
    tokens,
    norm_gain,
    query_weight,
    key_weight,
    value_weight,
    gate_weight,
    left_weight,
    input_weight,
    query_gain,
    key_gain,
    sink_logit,
    conv_weight,
    out_attention,
    out_conv,
):
    sp_count = lax.axis_size("sp")
    sp_place = lax.axis_index("sp")
    gathered = (
        lax.all_gather(query_weight, "sp", axis=1, tiled=True),
        lax.all_gather(key_weight, "sp", axis=1, tiled=True),
        lax.all_gather(value_weight, "sp", axis=1, tiled=True),
        lax.all_gather(gate_weight, "sp", axis=1, tiled=True),
        lax.all_gather(left_weight, "sp", axis=1, tiled=True),
        lax.all_gather(input_weight, "sp", axis=1, tiled=True),
        lax.all_gather(out_attention, "sp", axis=1, tiled=True),
        lax.all_gather(out_conv, "sp", axis=1, tiled=True),
    )
    (
        query_full,
        key_full,
        value_full,
        gate_full,
        left_full,
        input_full,
        attn_out_full,
        conv_out_full,
    ) = gathered
    normed = normalize(tokens.astype(jnp.float32), norm_gain).astype(jnp.bfloat16)
    widths = [
        query_full.shape[0],
        key_full.shape[0],
        value_full.shape[0],
        gate_full.shape[0],
        left_full.shape[0],
        input_full.shape[0],
    ]
    piece = lax.all_gather(normed, "tp", axis=0, tiled=True)
    joined = jnp.concatenate(
        [
            project(piece, weight)
            for weight in (query_full, key_full, value_full, gate_full, left_full, input_full)
        ],
        axis=1,
    )
    count = joined.shape[0]
    bounds = [0]
    for width in widths:
        bounds.append(bounds[-1] + width)
    query, keys, values, gate, left, inputs = [
        joined[:, bounds[place] : bounds[place + 1]] for place in range(6)
    ]
    offset = sp_place * count
    total = count * sp_count
    positions = (offset + jnp.arange(count, dtype=jnp.int32)).astype(jnp.float32)
    local_heads = widths[0] // HEAD_DIM
    kv_local = widths[1] // HEAD_DIM
    query_rot = rotate(
        normalize(query.reshape(count, local_heads, HEAD_DIM).astype(jnp.float32), query_gain),
        positions,
    ).astype(jnp.bfloat16)
    key_rot = rotate(
        normalize(keys.reshape(count, kv_local, HEAD_DIM).astype(jnp.float32), key_gain), positions
    ).astype(jnp.bfloat16)
    key_flat = key_rot.reshape(count, kv_local * HEAD_DIM)
    product = (left.astype(jnp.float32) * inputs.astype(jnp.float32)).astype(jnp.bfloat16)
    kv_width = widths[1]
    pair_rim = with_halo(jnp.concatenate([key_flat, values], axis=1), (("sp", 0),), WINDOW)
    product_rim = with_halo(product, (("sp", 0),), 1)
    rim_rows = pair_rim.shape[0]
    key_rim = pair_rim[:, :kv_width].reshape(rim_rows, kv_local, HEAD_DIM)
    value_rim = pair_rim[:, kv_width:].reshape(rim_rows, kv_local, HEAD_DIM)
    attended = attend(query_rot, key_rim, value_rim, sink_logit, offset, total)
    padded = product_rim.astype(jnp.float32)
    convolved = (
        conv_weight[0] * padded[:-2] + conv_weight[1] * padded[1:-1] + conv_weight[2] * padded[2:]
    )
    gated = (gate.astype(jnp.float32) * convolved).astype(jnp.bfloat16)
    return lax.psum_scatter(
        (
            jnp.dot(attended, attn_out_full, preferred_element_type=jnp.float32)
            + jnp.dot(gated, conv_out_full, preferred_element_type=jnp.float32)
        ).astype(jnp.bfloat16),
        "tp",
        scatter_dimension=0,
        tiled=True,
    )


MESH = pl.DeviceIdType.MESH


def fused_kernel(
    dims,
    tok_hbm, gain_hbm, q_hbm, k_hbm, v_hbm, g_hbm, l_hbm, i_hbm,
    qgain_hbm, kgain_hbm, sink_hbm, conv_hbm, oa_hbm, oc_hbm, trig_hbm,
    out_ref,
    gain_ref, qgain_ref, kgain_ref, sink_ref, conv_ref, tok, trig, stage, ostage, win, wout, normed, normed2, acc, acc2, rim, prod, prod2, mix_a, mix_c, gated2,
    qrot,
    keep, s1, r1, s2, r2,
    local_sem, y_send, w_recv, m_send, e_send,
    tok_send, tok_recv, tok2_send, tok2_recv, rim_send, rim_recv, prod_send, prod_recv, g_send, g_recv,
    rs_send, rs_recv,
):
    scope = jax.named_scope
    line, rows, depth, qr, kr, cr = (
        dims["line"], dims["rows"], dims["depth"], dims["qr"], dims["kr"], dims["cr"]
    )
    sp = lax.axis_index("sp")
    tp = lax.axis_index("tp")
    z, y = sp // 2, sp % 2
    x, c = tp // 2, tp % 2
    y_peer = (2 * z + 1 - y, tp)
    x_peer = (sp, 2 * (1 - x) + c)
    c_peer = (sp, 2 * x + 1 - c)
    low_side = z < 2
    toward = jnp.where(low_side, 1, -1)
    is_end = (z == 0) | (z == line - 1)
    inner = (z > 0) & (z < line - 1)
    m_plane = z + toward
    e_plane = jnp.where(inner, z - toward, m_plane)
    m_peer = (2 * m_plane + y, tp)
    e_peer = (2 * e_plane + y, tp)
    near = jnp.where(inner, z - toward, z + toward)
    mid = jnp.where(inner, z + toward, z + 2 * toward)
    far = jnp.where(inner, z + 2 * toward, z + 3 * toward)
    sources = (z, near, mid, far)
    s_own = sp
    s_mate = 2 * z + 1 - y
    plane = 8 * rows
    core = qr + 2 * kr

    barrier = pltpu.get_barrier_semaphore()
    for peer in (y_peer, x_peer, c_peer, m_peer):
        pl.semaphore_signal(barrier, inc=1, device_id=peer, device_id_type=MESH)

    @pl.when(inner)
    def _():
        pl.semaphore_signal(barrier, inc=1, device_id=e_peer, device_id_type=MESH)

    counter = [0]

    def local(src, dst):
        copy = pltpu.make_async_copy(src, dst, local_sem.at[counter[0]])
        counter[0] += 1
        copy.start()
        return copy

    def core_pieces(which, dst):
        q0 = pl.multiple_of(which * qr, qr)
        return [
            local(q_hbm.at[pl.ds(q0, qr)], dst.at[0:qr]),
            local(k_hbm, dst.at[qr : qr + kr]),
            local(v_hbm, dst.at[qr + kr : qr + 2 * kr]),
        ]

    def conv_pieces(which, dst):
        c0 = pl.multiple_of(which * cr, cr)
        return [
            local(g_hbm.at[pl.ds(c0, cr)], dst.at[core : core + cr]),
            local(l_hbm.at[pl.ds(c0, cr)], dst.at[core + cr : core + 2 * cr]),
            local(i_hbm.at[pl.ds(c0, cr)], dst.at[core + 2 * cr : core + 3 * cr]),
        ]

    def out_pieces(which, dst):
        q0, c0 = pl.multiple_of(which * qr, qr), pl.multiple_of(which * cr, cr)
        return [
            local(oa_hbm.at[pl.ds(q0, qr)], dst.at[0:qr]),
            local(oc_hbm.at[pl.ds(c0, cr)], dst.at[qr : qr + cr]),
        ]

    loads = core_pieces(y, win.at[s_own]) + core_pieces(1 - y, stage)
    tok_loads = [local(tok_hbm, tok), local(gain_hbm, gain_ref)]
    loads += conv_pieces(y, win.at[s_own]) + conv_pieces(1 - y, stage)
    loads += out_pieces(y, wout.at[s_own]) + out_pieces(1 - y, ostage)
    side_copies = [
        local(trig_hbm.at[pl.ds(pl.multiple_of(z * plane, plane), plane)], trig),
        local(qgain_hbm, qgain_ref),
        local(kgain_hbm, kgain_ref),
        local(sink_hbm, sink_ref),
        local(conv_hbm, conv_ref),
    ]

    with scope("barrier"):
        pl.semaphore_wait(barrier, 4 + inner.astype(jnp.int32))

    def remote(src, dst, send, recv, peer):
        return pltpu.make_async_remote_copy(
            src_ref=src, dst_ref=dst, send_sem=send, recv_sem=recv,
            device_id=peer, device_id_type=MESH,
        )

    def chunk(kind, s):
        if kind == 2:
            return wout.at[s]
        return win.at[s, 0:core] if kind == 0 else win.at[s, core : core + 3 * cr]

    def hop(kind, s, sends, peer):
        return remote(chunk(kind, s), chunk(kind, s), sends.at[kind, s], w_recv.at[kind, s], peer)

    def send_m(kind, s):
        hop(kind, s, m_send, m_peer).start()

    def send_e(kind, s):
        hop(kind, s, e_send, e_peer).start()

    def take(kind, s):
        hop(kind, s, m_send, m_peer).wait_recv()

    def y_hop(kind):
        if kind == 2:
            src = ostage
        else:
            src = stage.at[0:core] if kind == 0 else stage.at[core : core + 3 * cr]
        return remote(src, chunk(kind, s_own), y_send.at[kind], w_recv.at[kind, s_own], y_peer)

    def first_of(source):
        return 2 * source + y

    def second_of(source):
        return 2 * source + 1 - y

    for copy in loads:
        copy.wait()
    send_m(0, s_own)

    @pl.when(inner)
    def _():
        send_e(0, s_own)

    y_hop(0).start()

    @pl.when(inner)
    def _():
        send_m(1, s_own)
        send_e(2, s_own)

    with scope("norm"):
        for copy in tok_loads:
            copy.wait()
        t = tok[...].astype(jnp.float32)
        t = t * lax.rsqrt(jnp.mean(t * t, axis=-1, keepdims=True) + EPS) * gain_ref[...]

        def block_of(yy, xx, cc):
            return 4 * yy + 2 * xx + cc

        own_block = block_of(y, x, c)
        xb = block_of(y, 1 - x, c)
        yb = block_of(1 - y, x, c)
        db = block_of(1 - y, 1 - x, c)
        normed[own_block] = t.astype(jnp.bfloat16)

    def tok_hop(block, slot, peer):
        return remote(
            normed.at[block], normed.at[block], tok_send.at[slot], tok_recv.at[block], peer
        )

    def end_tok(block, slot, half=None):
        part = slice(0, rows) if half is None else slice(half * rows // 2, (half + 1) * rows // 2)
        return remote(
            normed.at[block, part], normed2.at[block, part], tok2_send.at[slot],
            tok2_recv.at[block], m_peer,
        )

    def tok2_hop(block, slot, peer):
        return remote(
            normed2.at[block], normed2.at[block], tok2_send.at[slot], tok2_recv.at[block], peer
        )

    tok_copies = []

    def tok_go(block, peer):
        copy = tok_hop(block, len(tok_copies), peer)
        copy.start()
        tok_copies.append(copy)

    def tok_wait(block):
        tok_hop(block, 0, x_peer).wait_recv()

    def tok2_wait(block):
        tok2_hop(block, 0, x_peer).wait_recv()

    @pl.when(is_end)
    def _():
        end_tok(own_block, 6, 0).start()

    tok_go(own_block, x_peer)
    tok_go(own_block, y_peer)
    tok_go(own_block, c_peer)
    y_hop(1).start()

    with scope("c_mate"):
        take(0, s_mate)
        send_m(0, s_mate)

        @pl.when(inner)
        def _():
            send_e(0, s_mate)
            take(0, first_of(near))
            send_m(0, first_of(near))
            take(0, first_of(mid))
            send_e(0, first_of(mid))

        @pl.when(is_end)
        def _():
            end_tok(own_block, 8, 1).start()
            send_m(1, s_own)

    with scope("tok_xb"):
        tok_wait(xb)
        tok_go(xb, c_peer)

    with scope("tok_yb"):
        tok_wait(yb)
        tok_go(yb, x_peer)
        tok_go(yb, c_peer)

    with scope("c_fwd"):
        @pl.when(inner)
        def _():
            take(0, second_of(mid))
            send_e(0, second_of(mid))
            take(0, second_of(near))
            send_m(0, second_of(near))

    with scope("tok2_own"):
        @pl.when(inner)
        def _():
            tok2_wait(own_block)
            tok2_hop(own_block, 0, x_peer).start()
            tok2_hop(own_block, 1, y_peer).start()
            tok2_hop(own_block, 2, c_peer).start()

    y_hop(2).start()

    with scope("v_mate"):
        take(1, s_mate)
        send_m(1, s_mate)

    with scope("far1"):
        @pl.when(inner)
        def _():
            take(0, first_of(far))
            send_e(0, first_of(far))

    with scope("tok_db"):
        tok_wait(db)
        tok_go(db, c_peer)

        @pl.when(is_end)
        def _():
            end_tok(db, 7).start()
            send_m(2, s_own)

    with scope("far2"):
        @pl.when(inner)
        def _():
            take(1, first_of(near))
            send_m(1, first_of(near))
            take(0, second_of(far))
            send_e(0, second_of(far))

    with scope("tok_rest"):
        for yy in range(2):
            for xx in range(2):
                tok_wait(block_of(yy, xx, 1 - c))

    def columns(s):
        return pl.ds(pl.multiple_of(s * depth, depth), depth)

    def dot_t(a, w):
        return lax.dot_general(a, w, (((1,), (1,)), ((), ())), preferred_element_type=jnp.float32)

    with scope("c_dots"):
        @pl.when(is_end)
        def _():
            for source in (near, mid, far):
                for s in (first_of(source), second_of(source)):
                    take(0, s)

        acc[:, 0:core] = jnp.zeros((plane, core), jnp.float32)

        def c_step(s, carry):
            a = normed[:, :, columns(s)].reshape(plane, depth)
            acc[:, 0:core] += dot_t(a, win[s, 0:core])
            return carry

        lax.fori_loop(0, 2 * line, c_step, 0)

    with scope("rot"):
        for copy in side_copies:
            copy.wait()
        lane = lax.broadcasted_iota(jnp.int32, (plane, qr), 1)
        half_dim = HEAD_DIM // 2
        table = trig[...]
        cos2 = jnp.where(lane < HEAD_DIM, table, pltpu.roll(table, HEAD_DIM, 1))
        sin2 = jnp.where(lane < HEAD_DIM, pltpu.roll(table, HEAD_DIM, 1), table)
        low = lane < HEAD_DIM
        first_half = lane % HEAD_DIM < half_dim

        def rot(v):
            partner = jnp.where(
                first_half, pltpu.roll(v, qr - half_dim, 1), pltpu.roll(v, half_dim, 1)
            )
            return v * cos2 + partner * sin2

        def bf(v):
            return v.astype(jnp.bfloat16).astype(jnp.float32)

        kv = bf(acc[:, qr : 2 * qr])
        ksq = jnp.sum(jnp.where(low, kv * kv, 0.0), axis=-1, keepdims=True) / HEAD_DIM
        kgain = jnp.concatenate([kgain_ref[...], kgain_ref[...]], axis=1)
        kn = kv * lax.rsqrt(ksq + EPS) * kgain
        krot = rot(kn)
        rim[WINDOW : WINDOW + plane, :] = jnp.where(low, krot, kv).astype(jnp.bfloat16)

    bottom = pl.ds(WINDOW, WINDOW)
    top = pl.ds(plane, WINDOW)
    up = (jnp.minimum(2 * (z + 1) + y, 2 * line - 1), tp)
    down = (jnp.maximum(2 * (z - 1) + y, 0), tp)
    has_up = z < line - 1
    has_down = z > 0
    rim_up = remote(rim.at[top], rim.at[pl.ds(0, WINDOW)], rim_send.at[0], rim_recv.at[0], up)
    rim_down = remote(
        rim.at[bottom], rim.at[pl.ds(WINDOW + plane, WINDOW)], rim_send.at[1], rim_recv.at[1], down
    )

    @pl.when(has_up)
    def _():
        rim_up.start()

    @pl.when(has_down)
    def _():
        rim_down.start()

    zero_rim = jnp.zeros((WINDOW, qr), jnp.bfloat16)

    @pl.when(z == 0)
    def _():
        rim[0:WINDOW] = zero_rim

    @pl.when(z == line - 1)
    def _():
        rim[WINDOW + plane :] = zero_rim

    with scope("v_near"):
        @pl.when(inner)
        def _():
            take(1, second_of(near))
            send_m(1, second_of(near))

    with scope("rotq"):
        qv = bf(acc[:, 0:qr])
        qq = qv * qv
        q_lo = jnp.sum(jnp.where(low, qq, 0.0), axis=-1, keepdims=True) / HEAD_DIM
        q_hi = jnp.sum(jnp.where(low, 0.0, qq), axis=-1, keepdims=True) / HEAD_DIM
        qgain = jnp.concatenate([qgain_ref[...], qgain_ref[...]], axis=1)
        qn = qv * lax.rsqrt(jnp.where(low, q_lo, q_hi) + EPS) * qgain
        qro = rot(qn)
        qrot[0] = jnp.where(low, qro, 0.0).astype(jnp.bfloat16)
        qrot[1] = jnp.where(low, pltpu.roll(qro, HEAD_DIM, 1), 0.0).astype(jnp.bfloat16)

    with scope("o_mate"):
        take(2, s_mate)

        @pl.when(is_end)
        def _():
            send_m(2, s_mate)

        @pl.when(inner)
        def _():
            send_m(2, 2 * z)
            send_m(2, 2 * z + 1)
            send_e(2, s_mate)
            for block, slot in ((xb, 3), (yb, 4)):
                tok2_wait(block)
                tok2_hop(block, slot, c_peer).start()

    span = BLOCK + 2 * WINDOW
    total = plane * line

    def att_block(block):
        begin = pl.multiple_of(block * BLOCK, BLOCK)
        kvb = rim[pl.ds(begin, span), :]
        qb = qrot[:, pl.ds(begin, BLOCK), :].reshape(2 * BLOCK, qr)
        scores = lax.dot_general(
            qb, kvb, (((1,), (1,)), ((), ())), preferred_element_type=jnp.float32
        ) * HEAD_DIM ** (-0.5)
        row = lax.broadcasted_iota(jnp.int32, (2 * BLOCK, span), 0)
        col = lax.broadcasted_iota(jnp.int32, (2 * BLOCK, span), 1)
        gap = row % BLOCK + WINDOW - col
        pos = z * plane + begin - WINDOW + col
        allowed = (gap <= WINDOW) & (gap >= -WINDOW) & (pos >= 0) & (pos < total)
        scores = jnp.where(allowed, scores, NEG_FILL)
        head = lax.broadcasted_iota(jnp.int32, (2 * BLOCK, 1), 0)
        sink = jnp.where(head < BLOCK, sink_ref[0, 2 * y], sink_ref[0, 2 * y + 1])
        peak = jnp.maximum(jnp.max(scores, axis=-1, keepdims=True), sink)
        expo = jnp.exp(scores - peak)
        denom = jnp.sum(expo, axis=-1, keepdims=True) + jnp.exp(sink - peak)
        weights = (expo / denom).astype(jnp.bfloat16)
        o = jnp.dot(weights, kvb, preferred_element_type=jnp.float32)
        low_b = lax.broadcasted_iota(jnp.int32, (BLOCK, qr), 1) < HEAD_DIM
        both = jnp.where(low_b, pltpu.roll(o[:BLOCK], HEAD_DIM, 1), o[BLOCK:])
        mix_a[pl.ds(begin, BLOCK), :] = both.astype(jnp.bfloat16)

    nblocks = plane // BLOCK

    def att_inner(block, carry):
        att_block(block)
        return carry

    with scope("att_in"):
        lax.fori_loop(1, nblocks - 1, att_inner, 0)

    def v_dot(s):
        a = normed[:, :, columns(s)].reshape(plane, depth)
        acc[:, core:] += dot_t(a, win[s, core:])

    def help_dot(s):
        a = normed2[:, :, columns(s)].reshape(plane, depth)
        acc2[...] += dot_t(a, win[s, core:])

    def early(k):
        source = jnp.where(k < 2, z, jnp.where(k < 4, near, mid))
        return 2 * source + k % 2

    with scope("tok2_side"):
        @pl.when(inner)
        def _():
            acc[:, core:] = jnp.zeros((plane, 3 * cr), jnp.float32)
            acc2[...] = jnp.zeros_like(acc2)
            for s in (first_of(mid), second_of(mid)):
                take(1, s)

    with scope("v_dots"):
        @pl.when(inner)
        def _():
            def v_step(k, carry):
                v_dot(early(k))
                return carry

            lax.fori_loop(0, 6, v_step, 0)

    with scope("rim_wait"):
        @pl.when(has_down)
        def _():
            rim_up.wait_recv()

        @pl.when(has_up)
        def _():
            rim_down.wait_recv()

    with scope("att_out"):
        def att_outer(k, carry):
            att_block(k * (nblocks - 1))
            return carry

        lax.fori_loop(0, 2, att_outer, 0)

    pad = 16
    zero_pad = jnp.zeros((pad, cr), jnp.bfloat16)
    taps = conv_ref[y]
    base = core

    def convolve(ref, gate):
        p = ref[...].astype(jnp.float32)
        before = pltpu.roll(p, 1, 0)[pad : pad + plane]
        after = pltpu.roll(p, plane + 2 * pad - 1, 0)[pad : pad + plane]
        mixed = taps[0:1] * before + taps[1:2] * p[pad : pad + plane] + taps[2:3] * after
        return (gate * mixed).astype(jnp.bfloat16)

    prod_up = remote(
        prod.at[pl.ds(plane, pad)], prod.at[pl.ds(0, pad)], prod_send.at[0], prod_recv.at[0], up
    )
    prod_down = remote(
        prod.at[pl.ds(pad, pad)], prod.at[pl.ds(pad + plane, pad)],
        prod_send.at[1], prod_recv.at[1], down,
    )
    low_inner = inner & low_side
    high_inner = inner & (z >= 2)
    g_copy = remote(gated2, mix_c, g_send.at[0], g_recv.at[0], e_peer)

    @pl.when(inner)
    def _():
        with scope("tok2_rest"):
            tok2_wait(db)
            tok2_hop(db, 5, c_peer).start()
            for yy in range(2):
                for xx in range(2):
                    tok2_wait(block_of(yy, xx, 1 - c))

        with scope("help_dots"):
            def help_step(k, carry):
                help_dot(early(k))
                return carry

            lax.fori_loop(0, 6, help_step, 0)

        with scope("far_dots"):
            for s in (first_of(far), second_of(far)):
                take(1, s)

            def far_step(k, carry):
                v_dot(2 * far + k)
                help_dot(2 * far + k)
                return carry

            lax.fori_loop(0, 2, far_step, 0)

        with scope("prod"):
            left = bf(acc[:, base + cr : base + 2 * cr])
            inputs = bf(acc[:, base + 2 * cr : base + 3 * cr])
            prod[pad : pad + plane] = (left * inputs).astype(jnp.bfloat16)

            @pl.when(low_inner)
            def _():
                prod_up.start()

            @pl.when(high_inner)
            def _():
                prod_down.start()

            take(2, first_of(near))
            send_m(2, first_of(near))

            prod2[pad : pad + plane] = (
                bf(acc2[:, cr : 2 * cr]) * bf(acc2[:, 2 * cr : 3 * cr])
            ).astype(jnp.bfloat16)

            @pl.when(z == 1)
            def _():
                prod2[0:pad] = zero_pad
                prod2[pad + plane :] = prod[pad : 2 * pad]
                prod[0:pad] = prod2[plane : plane + pad]

            @pl.when(z != 1)
            def _():
                prod2[0:pad] = prod[plane : plane + pad]
                prod2[pad + plane :] = zero_pad
                prod[pad + plane :] = prod2[pad : 2 * pad]

            gated2[...] = convolve(prod2, bf(acc2[:, 0:cr]))
            g_copy.start()

        with scope("o_fwd"):
            take(2, second_of(near))
            send_m(2, second_of(near))
            take(2, 2 * mid)
            send_e(2, 2 * mid)

        with scope("prod_wait"):
            @pl.when(low_inner)
            def _():
                prod_down.wait_recv()

            @pl.when(high_inner)
            def _():
                prod_up.wait_recv()

            mix_c[...] = convolve(prod, bf(acc[:, base : base + cr]))

    with scope("g_wait"):
        @pl.when(is_end)
        def _():
            g_copy.wait_recv()

    def group(cc):
        spans = [pl.ds(pl.multiple_of((2 * q + cc) * rows, rows), rows) for q in range(4)]
        return [jnp.concatenate([mix_a[w, :], mix_c[w, :]], axis=1) for w in spans]

    mine_rows = jnp.concatenate(group(c), axis=0)
    other_rows = jnp.concatenate(group(1 - c), axis=0)
    rs_copies = []

    def send_rs(src, dst, stage_id, s, peer):
        copy = remote(src, dst, rs_send.at[stage_id, s], rs_recv.at[stage_id, s], peer)
        copy.start()
        rs_copies.append(copy)

    def out_take(i):
        s = 2 * sources[i // 2] + i % 2
        take(2, s)

    def out_forward(i):
        s = 2 * sources[i // 2] + i % 2
        take(2, s)
        send_e(2, s)

    def stage_a(i):
        s = 2 * sources[i // 2] + i % 2
        weight = wout[s]
        s1[s] = jnp.dot(
            other_rows, weight, preferred_element_type=jnp.float32
        ).astype(jnp.bfloat16).reshape(2, 2, rows, depth)
        send_rs(s1.at[s], r1.at[s], 0, s, c_peer)
        keep[s] = jnp.dot(
            mine_rows, weight, preferred_element_type=jnp.float32
        ).reshape(2, 2, rows, depth)

    d_peer = (2 * z + 1 - y, 2 * (1 - x) + c)
    corners = ((1 - y, 1 - x, d_peer), (1 - y, x, y_peer), (y, 1 - x, x_peer))

    def stage_b(i):
        s = 2 * sources[i // 2] + i % 2
        remote(s1.at[s], r1.at[s], rs_send.at[0, s], rs_recv.at[0, s], c_peer).wait_recv()
        for j, (yy, xx, peer) in enumerate(corners):
            s2[s, j] = (keep[s, yy, xx] + r1[s, yy, xx].astype(jnp.float32)).astype(jnp.bfloat16)
            send_rs(s2.at[s, j], r2.at[s, j], 1 + j, s, peer)

    def stage_d(i):
        s = 2 * sources[i // 2] + i % 2
        part = keep[s, y, x] + r1[s, y, x].astype(jnp.float32)
        for j in (1, 2, 0):
            peer = corners[j][2]
            remote(
                s2.at[s, j], r2.at[s, j], rs_send.at[1 + j, s], rs_recv.at[1 + j, s], peer
            ).wait_recv()
        for j in range(3):
            part = part + r2[s, j].astype(jnp.float32)
        out_ref[:, columns(s)] = part.astype(jnp.bfloat16)

    order = (
        ("a", (0, 1, 2)), ("b", (0,)), ("a", (3,)), ("b", (1, 2, 3)), ("f", (5,)),
        ("w", (4,)), ("a", (4,)), ("b", (4,)), ("w", (5,)), ("a", (5,)), ("b", (5,)),
        ("f", (6,)), ("d", (0,)), ("f", (7,)), ("d", (1,)),
        ("w", (6,)), ("a", (6,)), ("b", (6,)), ("d", (2, 3)),
        ("w", (7,)), ("a", (7,)), ("b", (7,)), ("d", (4, 5, 6, 7)),
    )

    for step, places in order:
        for i in places:
            with scope(f"{step}{i}"):
                if step == "w":
                    pl.when(is_end)(functools.partial(out_take, i))
                elif step == "f":
                    pl.when(inner)(functools.partial(out_forward, i))
                elif step == "a":
                    if i in (2, 3):
                        pl.when(is_end)(functools.partial(out_take, i))
                    stage_a(i)
                elif step == "b":
                    stage_b(i)
                else:
                    stage_d(i)

    with scope("sends"):
        for kind in range(3):
            y_hop(kind).wait_send()
        for copy in tok_copies + rs_copies:
            copy.wait_send()

        @pl.when(has_up)
        def _():
            rim_up.wait_send()

        @pl.when(has_down)
        def _():
            rim_down.wait_send()

        for kind in range(3):
            for half in range(2):
                hop(kind, 2 * z + half, m_send, m_peer).wait_send()

        @pl.when(is_end)
        def _():
            end_tok(own_block, 6, 0).wait_send()
            end_tok(own_block, 8, 1).wait_send()
            end_tok(db, 7).wait_send()

        @pl.when(inner)
        def _():
            for slot in range(6):
                tok2_hop(own_block, slot, x_peer).wait_send()
            g_copy.wait_send()
            for half in range(2):
                for kind in range(3):
                    hop(kind, 2 * near + half, m_send, m_peer).wait_send()
                for source in (z, mid, far):
                    for kind in (0, 2):
                        hop(kind, 2 * source + half, e_send, e_peer).wait_send()

        @pl.when(low_inner)
        def _():
            prod_up.wait_send()

        @pl.when(high_inner)
        def _():
            prod_down.wait_send()


def trig_table(total):
    half = HEAD_DIM // 2
    freq = np.float64(ROPE_BASE) ** (-np.arange(half) / half)
    angle = np.arange(total)[:, None] * freq
    cosine, sine = np.cos(angle), np.sin(angle)
    return np.concatenate([cosine, cosine, -sine, sine], axis=1).astype(np.float32)


def fused_device(
    tokens, norm_gain, query_weight, key_weight, value_weight, gate_weight, left_weight,
    input_weight, query_gain, key_gain, sink_logit, conv_weight, out_attention, out_conv,
):
    sp_count = lax.axis_size("sp")
    line = sp_count // 2
    rows, width = tokens.shape
    depth = query_weight.shape[1]
    qr = query_weight.shape[0] // 2
    kr = key_weight.shape[0]
    cr = gate_weight.shape[0] // 2
    fan = qr + 2 * kr + 3 * cr
    plane = 8 * rows
    dims = dict(line=line, rows=rows, depth=depth, qr=qr, kr=kr, cr=cr)
    vm = pl.BlockSpec(memory_space=pltpu.VMEM)
    hb = pl.BlockSpec(memory_space=pl.ANY)
    bf16, f32 = jnp.bfloat16, jnp.float32
    dma = pltpu.SemaphoreType.DMA
    n = sp_count
    scratch = [
        pltpu.VMEM((1, width), f32),
        pltpu.VMEM((1, HEAD_DIM), f32),
        pltpu.VMEM((1, HEAD_DIM), f32),
        pltpu.SMEM((1, 4), f32),
        pltpu.VMEM((2, 3, cr), f32),
        pltpu.VMEM((rows, width), bf16),
        pltpu.VMEM((plane, 2 * HEAD_DIM), f32),
        pltpu.VMEM((fan, depth), bf16),
        pltpu.VMEM((qr + cr, depth), bf16),
        pltpu.VMEM((n, fan, depth), bf16),
        pltpu.VMEM((n, qr + cr, depth), bf16),
        pltpu.VMEM((8, rows, width), bf16),
        pltpu.VMEM((8, rows, width), bf16),
        pltpu.VMEM((plane, fan), f32),
        pltpu.VMEM((plane, 3 * cr), f32),
        pltpu.VMEM((plane + 2 * WINDOW, qr), bf16),
        pltpu.VMEM((plane + 32, cr), bf16),
        pltpu.VMEM((plane + 32, cr), bf16),
        pltpu.VMEM((plane, qr), bf16),
        pltpu.VMEM((plane, cr), bf16),
        pltpu.VMEM((plane, cr), bf16),
        pltpu.VMEM((2, plane, qr), bf16),
        pltpu.VMEM((n, 2, 2, rows, depth), f32),
        pltpu.VMEM((n, 2, 2, rows, depth), bf16),
        pltpu.VMEM((n, 2, 2, rows, depth), bf16),
        pltpu.VMEM((n, 3, rows, depth), bf16),
        pltpu.VMEM((n, 3, rows, depth), bf16),
        dma((23,)), dma((3,)), dma((3, n)), dma((3, n)), dma((3, n)),
        dma((7,)), dma((8,)), dma((9,)), dma((8,)), dma((2,)), dma((2,)), dma((2,)), dma((2,)),
        dma((1,)), dma((1,)), dma((4, n)), dma((4, n)),
    ]
    taps = conv_weight.reshape(3, 2, cr).transpose(1, 0, 2)
    return pl.pallas_call(
        functools.partial(fused_kernel, dims),
        out_shape=jax.ShapeDtypeStruct((rows, width), bf16),
        in_specs=[hb] * 15,
        out_specs=vm,
        scratch_shapes=scratch,
        compiler_params=pltpu.CompilerParams(
            collective_id=0, has_side_effects=True, vmem_limit_bytes=56 * 1024 * 1024
        ),
    )(
        tokens, norm_gain[None, :], query_weight, key_weight, value_weight, gate_weight,
        left_weight, input_weight, query_gain[None, :],
        key_gain[None, :], sink_logit[None, :], taps, out_attention, out_conv,
        jnp.asarray(trig_table(plane * line)),
    )


def local_device(*args):
    tokens, query_weight, key_weight, gate_weight = args[0], args[2], args[3], args[5]
    fits = (
        lax.axis_size("sp") == 8
        and lax.axis_size("tp") == 4
        and query_weight.shape[1] % 128 == 0
        and query_weight.shape[0] == 4 * HEAD_DIM
        and key_weight.shape[0] == HEAD_DIM
        and gate_weight.shape[0] == 256
        and tokens.shape[0] % 16 == 0
        and 8 * tokens.shape[0] % BLOCK == 0
        and 8 * tokens.shape[0] >= 2 * BLOCK
    )
    return fused_device(*args) if fits else per_device(*args)


def solution(mesh):
    in_specs = (
        P(("sp", "tp"), None),
        P(),
        P("tp", "sp"),
        P("tp", "sp"),
        P("tp", "sp"),
        P("tp", "sp"),
        P("tp", "sp"),
        P("tp", "sp"),
        P(),
        P(),
        P("tp"),
        P(None, "tp"),
        P("tp", "sp"),
        P("tp", "sp"),
    )
    out_specs = P(("sp", "tp"), None)
    return jax.shard_map(
        local_device, mesh=mesh, in_specs=in_specs, out_specs=out_specs, check_vma=False
    )
```

time: 82.8 us -> 66.6 us (0.80)
  Pallas kernels: 80.9 us -> 64.8 us
    pallas_call x1, Pallas kernels: 80.9 us -> 64.8 us  [fused_device(): pl.pallas_call(functools.partial(fused_kernel, dims), out_shape=jax.Shape...]
where the time goes in v1:
time: 66.6 us; the launch traced here: 66.4 us
  Pallas kernels  64.8 us (97%)
  local copies, waits for them, and re-layouts  1.67 us (3%)
    pallas_call x1, Pallas kernels, fused_device(): pl.pallas_call(functools.partial(fused_kernel, dims), out_shape=jax.Shape...  64.8 us
    unnamed x1, local copies, waits for them, and re-layouts  1.67 us

profile of v1, /device:TPU:0, one launch (start us, length us, event | category | flops | bytes accessed | tf_op | source)
XLA Modules:
  0.0 66.4 jit_solution(8812847954836976834)
XLA Ops:
  0.0 64.8 %shard_map.145 = bf16[64,2048]{1,0:T(8,128)(2,1)} custom-call(bf16[64,2048]{1,0:T(8,128)(2,1)} %tok_hbm.1, f32[1,2048]{1,0:T(1,128)} %bitcast.7, bf16[256,256]{1,0:T(8,128)(2,1)} %q_hbm.1, bf16[64,256]{1,0:T(8,128)(2,1)} %k_hbm.1, bf16[64,256]{1,0:T(8,128)(2,1)} %v_hbm.1, bf16[256,256]{1,0:T(8,128)(2,1)} %g_hbm.1, bf16[256,256]{1,0:T(8,128)(2,1)} %l_hbm.1, ...), custom_call_target="tpu_custom_call" | custom-call | tf_op jit(solution)/shard_map/pallas_call | solution.py:959
  64.8 1.7 %copy.17 = bf16[64,2048]{1,0:T(8,128)(2,1)} copy(bf16[64,2048]{1,0:T(8,128)(2,1)} %shard_map.145) | data formatting | bytes 524288

commit v2 on v1

--- a/solution.py
+++ b/solution.py
@@ -299,8 +299,8 @@
         )
 
     def chunk(kind, s):
-        if kind == 2:
-            return wout.at[s]
+        if kind > 1:
+            return wout.at[s, 0:qr] if kind == 2 else wout.at[s, qr : qr + cr]
         return win.at[s, 0:core] if kind == 0 else win.at[s, core : core + 3 * cr]
 
     def hop(kind, s, sends, peer):
@@ -316,12 +316,22 @@
         hop(kind, s, m_send, m_peer).wait_recv()
 
     def y_hop(kind):
-        if kind == 2:
-            src = ostage
+        if kind > 1:
+            src = ostage.at[0:qr] if kind == 2 else ostage.at[qr : qr + cr]
         else:
             src = stage.at[0:core] if kind == 0 else stage.at[core : core + 3 * cr]
         return remote(src, chunk(kind, s_own), y_send.at[kind], w_recv.at[kind, s_own], y_peer)
 
+    def out_hop(s, *sends):
+        for kind in (2, 3):
+            take(kind, s)
+            for send in sends:
+                send(kind, s)
+
+    def out_send(s, send):
+        send(2, s)
+        send(3, s)
+
     def first_of(source):
         return 2 * source + y
 
@@ -341,7 +351,7 @@
     @pl.when(inner)
     def _():
         send_m(1, s_own)
-        send_e(2, s_own)
+        out_send(s_own, send_e)
 
     with scope("norm"):
         for copy in tok_loads:
@@ -358,44 +368,48 @@
         db = block_of(1 - y, 1 - x, c)
         normed[own_block] = t.astype(jnp.bfloat16)
 
-    def tok_hop(block, slot, peer):
+    def part(ref, block, half):
+        if half == 2:
+            return ref.at[block]
+        return ref.at[block, half * rows // 2 : (half + 1) * rows // 2]
+
+    def tok_hop(block, half, slot, peer):
+        here = part(normed, block, half)
+        return remote(here, here, tok_send.at[slot], tok_recv.at[half, block], peer)
+
+    def end_tok(block, half, slot):
         return remote(
-            normed.at[block], normed.at[block], tok_send.at[slot], tok_recv.at[block], peer
+            part(normed, block, half), part(normed2, block, half), tok2_send.at[slot],
+            tok2_recv.at[half, block], m_peer,
         )
 
-    def end_tok(block, slot, half=None):
-        part = slice(0, rows) if half is None else slice(half * rows // 2, (half + 1) * rows // 2)
-        return remote(
-            normed.at[block, part], normed2.at[block, part], tok2_send.at[slot],
-            tok2_recv.at[block], m_peer,
-        )
-
-    def tok2_hop(block, slot, peer):
-        return remote(
-            normed2.at[block], normed2.at[block], tok2_send.at[slot], tok2_recv.at[block], peer
-        )
+    def tok2_hop(block, half, slot, peer):
+        here = part(normed2, block, half)
+        return remote(here, here, tok2_send.at[slot], tok2_recv.at[half, block], peer)
 
     tok_copies = []
 
-    def tok_go(block, peer):
-        copy = tok_hop(block, len(tok_copies), peer)
+    def tok_go(block, half, peer):
+        copy = tok_hop(block, half, len(tok_copies), peer)
         copy.start()
         tok_copies.append(copy)
 
-    def tok_wait(block):
-        tok_hop(block, 0, x_peer).wait_recv()
-
-    def tok2_wait(block):
-        tok2_hop(block, 0, x_peer).wait_recv()
+    def tok_wait(block, half):
+        tok_hop(block, half, 0, x_peer).wait_recv()
+
+    def tok2_wait(block, half):
+        tok2_hop(block, half, 0, x_peer).wait_recv()
 
     @pl.when(is_end)
     def _():
-        end_tok(own_block, 6, 0).start()
-
-    tok_go(own_block, x_peer)
-    tok_go(own_block, y_peer)
-    tok_go(own_block, c_peer)
+        end_tok(own_block, 0, 6).start()
+
+    tok_go(own_block, 1, x_peer)
+    tok_go(own_block, 0, y_peer)
+    tok_go(own_block, 0, x_peer)
+    tok_go(own_block, 1, y_peer)
     y_hop(1).start()
+    tok_go(own_block, 2, c_peer)
 
     with scope("c_mate"):
         take(0, s_mate)
@@ -411,17 +425,18 @@
 
         @pl.when(is_end)
         def _():
-            end_tok(own_block, 8, 1).start()
+            end_tok(own_block, 1, 7).start()
             send_m(1, s_own)
 
-    with scope("tok_xb"):
-        tok_wait(xb)
-        tok_go(xb, c_peer)
-
-    with scope("tok_yb"):
-        tok_wait(yb)
-        tok_go(yb, x_peer)
-        tok_go(yb, c_peer)
+    with scope("tok_xy"):
+        tok_wait(xb, 1)
+        tok_go(xb, 1, y_peer)
+        tok_wait(yb, 0)
+        tok_go(yb, 0, x_peer)
+        tok_wait(xb, 0)
+        tok_go(xb, 2, c_peer)
+        tok_wait(yb, 1)
+        tok_go(yb, 2, c_peer)
 
     with scope("c_fwd"):
         @pl.when(inner)
@@ -434,50 +449,78 @@
     with scope("tok2_own"):
         @pl.when(inner)
         def _():
-            tok2_wait(own_block)
-            tok2_hop(own_block, 0, x_peer).start()
-            tok2_hop(own_block, 1, y_peer).start()
-            tok2_hop(own_block, 2, c_peer).start()
+            tok2_wait(own_block, 0)
+            tok2_wait(own_block, 1)
+            tok2_hop(own_block, 2, 0, x_peer).start()
+            tok2_hop(own_block, 2, 1, y_peer).start()
+            tok2_hop(own_block, 2, 2, c_peer).start()
 
     y_hop(2).start()
+    y_hop(3).start()
+
+    with scope("far1"):
+        @pl.when(inner)
+        def _():
+            take(0, first_of(far))
+            send_e(0, first_of(far))
 
     with scope("v_mate"):
         take(1, s_mate)
         send_m(1, s_mate)
 
-    with scope("far1"):
-        @pl.when(inner)
-        def _():
-            take(0, first_of(far))
-            send_e(0, first_of(far))
+    with scope("far2"):
+        @pl.when(inner)
+        def _():
+            take(0, second_of(far))
+            send_e(0, second_of(far))
 
     with scope("tok_db"):
-        tok_wait(db)
-        tok_go(db, c_peer)
+        tok_wait(db, 0)
+        tok_wait(db, 1)
+        tok_go(db, 2, c_peer)
 
         @pl.when(is_end)
         def _():
-            end_tok(db, 7).start()
-            send_m(2, s_own)
-
-    with scope("far2"):
+            end_tok(db, 0, 8).start()
+            end_tok(db, 1, 9).start()
+
+    with scope("v_near1"):
         @pl.when(inner)
         def _():
             take(1, first_of(near))
             send_m(1, first_of(near))
-            take(0, second_of(far))
-            send_e(0, second_of(far))
 
     with scope("tok_rest"):
         for yy in range(2):
             for xx in range(2):
-                tok_wait(block_of(yy, xx, 1 - c))
+                tok_wait(block_of(yy, xx, 1 - c), 2)
 
     def columns(s):
         return pl.ds(pl.multiple_of(s * depth, depth), depth)
 
     def dot_t(a, w):
         return lax.dot_general(a, w, (((1,), (1,)), ((), ())), preferred_element_type=jnp.float32)
+
+    def plane_dots(tokens, into, cols, weight_rows, source, add):
+        total = into[:, cols] if add else None
+        for half in range(2):
+            s = 2 * source + half
+            a = tokens[:, :, columns(s)].reshape(plane, depth)
+            product = dot_t(a, win[s, weight_rows])
+            total = product if total is None else total + product
+        into[:, cols] = total
+
+    conv_rows = slice(core, core + 3 * cr)
+
+    def early_dots(tokens, into, cols, weight_rows, count):
+        plane_dots(tokens, into, cols, weight_rows, z, False)
+
+        def step(k, carry):
+            source = jnp.where(k == 1, near, jnp.where(k == 2, mid, far))
+            plane_dots(tokens, into, cols, weight_rows, source, True)
+            return carry
+
+        lax.fori_loop(1, count, step, 0)
 
     with scope("c_dots"):
         @pl.when(is_end)
@@ -486,14 +529,7 @@
                 for s in (first_of(source), second_of(source)):
                     take(0, s)
 
-        acc[:, 0:core] = jnp.zeros((plane, core), jnp.float32)
-
-        def c_step(s, carry):
-            a = normed[:, :, columns(s)].reshape(plane, depth)
-            acc[:, 0:core] += dot_t(a, win[s, 0:core])
-            return carry
-
-        lax.fori_loop(0, 2 * line, c_step, 0)
+        early_dots(normed, acc, slice(0, core), slice(0, core), line)
 
     with scope("rot"):
         for copy in side_copies:
@@ -551,12 +587,6 @@
     def _():
         rim[WINDOW + plane :] = zero_rim
 
-    with scope("v_near"):
-        @pl.when(inner)
-        def _():
-            take(1, second_of(near))
-            send_m(1, second_of(near))
-
     with scope("rotq"):
         qv = bf(acc[:, 0:qr])
         qq = qv * qv
@@ -568,21 +598,11 @@
         qrot[0] = jnp.where(low, qro, 0.0).astype(jnp.bfloat16)
         qrot[1] = jnp.where(low, pltpu.roll(qro, HEAD_DIM, 1), 0.0).astype(jnp.bfloat16)
 
-    with scope("o_mate"):
-        take(2, s_mate)
-
-        @pl.when(is_end)
-        def _():
-            send_m(2, s_mate)
-
-        @pl.when(inner)
-        def _():
-            send_m(2, 2 * z)
-            send_m(2, 2 * z + 1)
-            send_e(2, s_mate)
-            for block, slot in ((xb, 3), (yb, 4)):
-                tok2_wait(block)
-                tok2_hop(block, slot, c_peer).start()
+    with scope("tok2_xb"):
+        @pl.when(inner)
+        def _():
+            tok2_wait(xb, 2)
+            tok2_hop(xb, 2, 3, c_peer).start()
 
     span = BLOCK + 2 * WINDOW
     total = plane * line
@@ -620,50 +640,63 @@
     with scope("att_in"):
         lax.fori_loop(1, nblocks - 1, att_inner, 0)
 
-    def v_dot(s):
-        a = normed[:, :, columns(s)].reshape(plane, depth)
-        acc[:, core:] += dot_t(a, win[s, core:])
-
-    def help_dot(s):
-        a = normed2[:, :, columns(s)].reshape(plane, depth)
-        acc2[...] += dot_t(a, win[s, core:])
-
-    def early(k):
-        source = jnp.where(k < 2, z, jnp.where(k < 4, near, mid))
-        return 2 * source + k % 2
-
-    with scope("tok2_side"):
-        @pl.when(inner)
-        def _():
-            acc[:, core:] = jnp.zeros((plane, 3 * cr), jnp.float32)
-            acc2[...] = jnp.zeros_like(acc2)
+    with scope("tok2_yb"):
+        @pl.when(inner)
+        def _():
+            tok2_wait(yb, 2)
+            tok2_hop(yb, 2, 4, c_peer).start()
+
+    with scope("v_near2"):
+        @pl.when(inner)
+        def _():
+            take(1, second_of(near))
+            send_m(1, second_of(near))
+
+    with scope("o_mate"):
+        @pl.when(is_end)
+        def _():
+            out_send(s_own, send_m)
+            out_hop(s_mate, send_m)
+
+        @pl.when(inner)
+        def _():
+            out_send(s_own, send_m)
+            out_hop(s_mate, send_e)
+
+    with scope("v_mid"):
+        @pl.when(inner)
+        def _():
             for s in (first_of(mid), second_of(mid)):
                 take(1, s)
 
     with scope("v_dots"):
         @pl.when(inner)
         def _():
-            def v_step(k, carry):
-                v_dot(early(k))
+            early_dots(normed, acc, conv_rows, conv_rows, 3)
+
+    with scope("tok2_db"):
+        @pl.when(inner)
+        def _():
+            tok2_wait(db, 0)
+            tok2_wait(db, 1)
+            tok2_hop(db, 2, 5, c_peer).start()
+
+    def attend_edges():
+        with scope("rim_wait"):
+            @pl.when(has_down)
+            def _():
+                rim_up.wait_recv()
+
+            @pl.when(has_up)
+            def _():
+                rim_down.wait_recv()
+
+        with scope("att_out"):
+            def att_outer(k, carry):
+                att_block(k * (nblocks - 1))
                 return carry
 
-            lax.fori_loop(0, 6, v_step, 0)
-
-    with scope("rim_wait"):
-        @pl.when(has_down)
-        def _():
-            rim_up.wait_recv()
-
-        @pl.when(has_up)
-        def _():
-            rim_down.wait_recv()
-
-    with scope("att_out"):
-        def att_outer(k, carry):
-            att_block(k * (nblocks - 1))
-            return carry
-
-        lax.fori_loop(0, 2, att_outer, 0)
+            lax.fori_loop(0, 2, att_outer, 0)
 
     pad = 16
     zero_pad = jnp.zeros((pad, cr), jnp.bfloat16)
@@ -691,29 +724,18 @@
     @pl.when(inner)
     def _():
         with scope("tok2_rest"):
-            tok2_wait(db)
-            tok2_hop(db, 5, c_peer).start()
             for yy in range(2):
                 for xx in range(2):
-                    tok2_wait(block_of(yy, xx, 1 - c))
+                    tok2_wait(block_of(yy, xx, 1 - c), 2)
 
         with scope("help_dots"):
-            def help_step(k, carry):
-                help_dot(early(k))
-                return carry
-
-            lax.fori_loop(0, 6, help_step, 0)
+            early_dots(normed2, acc2, slice(0, 3 * cr), conv_rows, 3)
 
         with scope("far_dots"):
             for s in (first_of(far), second_of(far)):
                 take(1, s)
-
-            def far_step(k, carry):
-                v_dot(2 * far + k)
-                help_dot(2 * far + k)
-                return carry
-
-            lax.fori_loop(0, 2, far_step, 0)
+            plane_dots(normed2, acc2, slice(0, 3 * cr), conv_rows, far, True)
+            plane_dots(normed, acc, conv_rows, conv_rows, far, True)
 
         with scope("prod"):
             left = bf(acc[:, base + cr : base + 2 * cr])
@@ -728,8 +750,8 @@
             def _():
                 prod_down.start()
 
-            take(2, first_of(near))
-            send_m(2, first_of(near))
+            out_send(s_mate, send_m)
+            out_hop(first_of(near), send_m)
 
             prod2[pad : pad + plane] = (
                 bf(acc2[:, cr : 2 * cr]) * bf(acc2[:, 2 * cr : 3 * cr])
@@ -750,11 +772,11 @@
             gated2[...] = convolve(prod2, bf(acc2[:, 0:cr]))
             g_copy.start()
 
+        attend_edges()
+
         with scope("o_fwd"):
-            take(2, second_of(near))
-            send_m(2, second_of(near))
-            take(2, 2 * mid)
-            send_e(2, 2 * mid)
+            out_hop(second_of(near), send_m)
+            out_hop(first_of(mid), send_e)
 
         with scope("prod_wait"):
             @pl.when(low_inner)
@@ -767,9 +789,10 @@
 
             mix_c[...] = convolve(prod, bf(acc[:, base : base + cr]))
 
-    with scope("g_wait"):
-        @pl.when(is_end)
-        def _():
+    @pl.when(is_end)
+    def _():
+        attend_edges()
+        with scope("g_wait"):
             g_copy.wait_recv()
 
     def group(cc):
@@ -787,12 +810,11 @@
 
     def out_take(i):
         s = 2 * sources[i // 2] + i % 2
-        take(2, s)
+        out_hop(s)
 
     def out_forward(i):
-        s = 2 * sources[i // 2] + i % 2
-        take(2, s)
-        send_e(2, s)
+        source = sources[i // 2]
+        out_hop(first_of(source) if i % 2 == 0 else second_of(source), send_e)
 
     def stage_a(i):
         s = 2 * sources[i // 2] + i % 2
@@ -817,22 +839,22 @@
 
     def stage_d(i):
         s = 2 * sources[i // 2] + i % 2
-        part = keep[s, y, x] + r1[s, y, x].astype(jnp.float32)
+        piece = keep[s, y, x] + r1[s, y, x].astype(jnp.float32)
         for j in (1, 2, 0):
             peer = corners[j][2]
             remote(
                 s2.at[s, j], r2.at[s, j], rs_send.at[1 + j, s], rs_recv.at[1 + j, s], peer
             ).wait_recv()
         for j in range(3):
-            part = part + r2[s, j].astype(jnp.float32)
-        out_ref[:, columns(s)] = part.astype(jnp.bfloat16)
+            piece = piece + r2[s, j].astype(jnp.float32)
+        out_ref[:, columns(s)] = piece.astype(jnp.bfloat16)
 
     order = (
-        ("a", (0, 1, 2)), ("b", (0,)), ("a", (3,)), ("b", (1, 2, 3)), ("f", (5,)),
-        ("w", (4,)), ("a", (4,)), ("b", (4,)), ("w", (5,)), ("a", (5,)), ("b", (5,)),
-        ("f", (6,)), ("d", (0,)), ("f", (7,)), ("d", (1,)),
-        ("w", (6,)), ("a", (6,)), ("b", (6,)), ("d", (2, 3)),
-        ("w", (7,)), ("a", (7,)), ("b", (7,)), ("d", (4, 5, 6, 7)),
+        ("a", (0, 1)), ("f", (5,)), ("b", (0,)), ("a", (2,)), ("b", (1,)), ("a", (3,)),
+        ("b", (2, 3)), ("w", (4,)), ("a", (4,)), ("f", (6,)), ("b", (4,)),
+        ("w", (5,)), ("a", (5,)), ("b", (5,)), ("f", (7,)), ("w", (6,)), ("a", (6,)), ("b", (6,)),
+        ("d", (0, 1)), ("w", (7,)), ("a", (7,)), ("b", (7,)),
+        ("d", (2, 3, 4, 5, 6, 7)),
     )
 
     for step, places in order:
@@ -852,7 +874,7 @@
                     stage_d(i)
 
     with scope("sends"):
-        for kind in range(3):
+        for kind in range(4):
             y_hop(kind).wait_send()
         for copy in tok_copies + rs_copies:
             copy.wait_send()
@@ -865,26 +887,26 @@
         def _():
             rim_down.wait_send()
 
-        for kind in range(3):
+        for kind in range(4):
             for half in range(2):
                 hop(kind, 2 * z + half, m_send, m_peer).wait_send()
 
         @pl.when(is_end)
         def _():
-            end_tok(own_block, 6, 0).wait_send()
-            end_tok(own_block, 8, 1).wait_send()
-            end_tok(db, 7).wait_send()
+            for half in range(2):
+                end_tok(own_block, half, 6 + half).wait_send()
+                end_tok(db, half, 8 + half).wait_send()
 
         @pl.when(inner)
         def _():
             for slot in range(6):
-                tok2_hop(own_block, slot, x_peer).wait_send()
+                tok2_hop(own_block, 2, slot, x_peer).wait_send()
             g_copy.wait_send()
             for half in range(2):
-                for kind in range(3):
+                for kind in range(4):
                     hop(kind, 2 * near + half, m_send, m_peer).wait_send()
                 for source in (z, mid, far):
-                    for kind in (0, 2):
+                    for kind in (0, 2, 3):
                         hop(kind, 2 * source + half, e_send, e_peer).wait_send()
 
         @pl.when(low_inner)
@@ -951,8 +973,8 @@
         pltpu.VMEM((n, 2, 2, rows, depth), bf16),
         pltpu.VMEM((n, 3, rows, depth), bf16),
         pltpu.VMEM((n, 3, rows, depth), bf16),
-        dma((23,)), dma((3,)), dma((3, n)), dma((3, n)), dma((3, n)),
-        dma((7,)), dma((8,)), dma((9,)), dma((8,)), dma((2,)), dma((2,)), dma((2,)), dma((2,)),
+        dma((23,)), dma((4,)), dma((4, n)), dma((4, n)), dma((4, n)),
+        dma((10,)), dma((3, 8)), dma((10,)), dma((3, 8)), dma((2,)), dma((2,)), dma((2,)), dma((2,)),
         dma((1,)), dma((1,)), dma((4, n)), dma((4, n)),
     ]
     taps = conv_weight.reshape(3, 2, cr).transpose(1, 0, 2)
@@ -982,7 +1004,7 @@
         and query_weight.shape[0] == 4 * HEAD_DIM
         and key_weight.shape[0] == HEAD_DIM
         and gate_weight.shape[0] == 256
-        and tokens.shape[0] % 16 == 0
+        and tokens.shape[0] % 32 == 0
         and 8 * tokens.shape[0] % BLOCK == 0
         and 8 * tokens.shape[0] >= 2 * BLOCK
     )

time: 66.6 us -> 62.6 us (0.940)
  Pallas kernels: 64.8 us -> 60.7 us
    pallas_call x1, Pallas kernels: 64.8 us -> 60.7 us  [fused_device(): pl.pallas_call(functools.partial(fused_kernel, dims), out_shape=jax.Shape...]
where the time goes in v2:
time: 62.6 us; the launch traced here: 62.4 us
  Pallas kernels  60.7 us (97%)
  local copies, waits for them, and re-layouts  1.67 us (3%)
    pallas_call x1, Pallas kernels, fused_device(): pl.pallas_call(functools.partial(fused_kernel, dims), out_shape=jax.Shape...  60.7 us
    unnamed x1, local copies, waits for them, and re-layouts  1.67 us

profile of v2, /device:TPU:0, one launch (start us, length us, event | category | flops | bytes accessed | tf_op | source)
XLA Modules:
  0.0 62.4 jit_solution(13143643195088668298)
XLA Ops:
  0.0 60.7 %shard_map.145 = bf16[64,2048]{1,0:T(8,128)(2,1)} custom-call(bf16[64,2048]{1,0:T(8,128)(2,1)} %tok_hbm.1, f32[1,2048]{1,0:T(1,128)} %bitcast.7, bf16[256,256]{1,0:T(8,128)(2,1)} %q_hbm.1, bf16[64,256]{1,0:T(8,128)(2,1)} %k_hbm.1, bf16[64,256]{1,0:T(8,128)(2,1)} %v_hbm.1, bf16[256,256]{1,0:T(8,128)(2,1)} %g_hbm.1, bf16[256,256]{1,0:T(8,128)(2,1)} %l_hbm.1, ...), custom_call_target="tpu_custom_call" | custom-call | tf_op jit(solution)/shard_map/pallas_call | solution.py:981
  60.7 1.7 %copy.17 = bf16[64,2048]{1,0:T(8,128)(2,1)} copy(bf16[64,2048]{1,0:T(8,128)(2,1)} %shard_map.145) | data formatting | bytes 524288

commit v3 on v2

--- a/solution.py
+++ b/solution.py
@@ -246,47 +246,36 @@
     def _():
         pl.semaphore_signal(barrier, inc=1, device_id=e_peer, device_id_type=MESH)
 
-    counter = [0]
-
-    def local(src, dst):
-        copy = pltpu.make_async_copy(src, dst, local_sem.at[counter[0]])
-        counter[0] += 1
+    def local(src, dst, place):
+        copy = pltpu.make_async_copy(src, dst, local_sem.at[place])
         copy.start()
         return copy
 
-    def core_pieces(which, dst):
-        q0 = pl.multiple_of(which * qr, qr)
-        return [
-            local(q_hbm.at[pl.ds(q0, qr)], dst.at[0:qr]),
-            local(k_hbm, dst.at[qr : qr + kr]),
-            local(v_hbm, dst.at[qr + kr : qr + 2 * kr]),
-        ]
-
-    def conv_pieces(which, dst):
-        c0 = pl.multiple_of(which * cr, cr)
-        return [
-            local(g_hbm.at[pl.ds(c0, cr)], dst.at[core : core + cr]),
-            local(l_hbm.at[pl.ds(c0, cr)], dst.at[core + cr : core + 2 * cr]),
-            local(i_hbm.at[pl.ds(c0, cr)], dst.at[core + 2 * cr : core + 3 * cr]),
-        ]
-
-    def out_pieces(which, dst):
+    def in_pieces(which, dst, place):
         q0, c0 = pl.multiple_of(which * qr, qr), pl.multiple_of(which * cr, cr)
-        return [
-            local(oa_hbm.at[pl.ds(q0, qr)], dst.at[0:qr]),
-            local(oc_hbm.at[pl.ds(c0, cr)], dst.at[qr : qr + cr]),
-        ]
-
-    loads = core_pieces(y, win.at[s_own]) + core_pieces(1 - y, stage)
-    tok_loads = [local(tok_hbm, tok), local(gain_hbm, gain_ref)]
-    loads += conv_pieces(y, win.at[s_own]) + conv_pieces(1 - y, stage)
-    loads += out_pieces(y, wout.at[s_own]) + out_pieces(1 - y, ostage)
+        local(q_hbm.at[pl.ds(q0, qr)], dst.at[0:qr], place)
+        local(k_hbm, dst.at[qr : qr + kr], place)
+        local(v_hbm, dst.at[qr + kr : core], place)
+        for turn, ref in enumerate((g_hbm, l_hbm, i_hbm)):
+            lo = core + turn * cr
+            local(ref.at[pl.ds(c0, cr)], dst.at[lo : lo + cr], place)
+        return pltpu.make_async_copy(dst, dst, local_sem.at[place])
+
+    def out_pieces(which, dst, place):
+        q0, c0 = pl.multiple_of(which * qr, qr), pl.multiple_of(which * cr, cr)
+        local(oa_hbm.at[pl.ds(q0, qr)], dst.at[0:qr], place)
+        local(oc_hbm.at[pl.ds(c0, cr)], dst.at[qr : qr + cr], place)
+        return pltpu.make_async_copy(dst, dst, local_sem.at[place])
+
+    loads = [in_pieces(y, win.at[s_own], 0), in_pieces(1 - y, stage, 1)]
+    tok_loads = [local(tok_hbm, tok, 2), local(gain_hbm, gain_ref, 3)]
+    loads += [out_pieces(y, wout.at[s_own], 4), out_pieces(1 - y, ostage, 5)]
     side_copies = [
-        local(trig_hbm.at[pl.ds(pl.multiple_of(z * plane, plane), plane)], trig),
-        local(qgain_hbm, qgain_ref),
-        local(kgain_hbm, kgain_ref),
-        local(sink_hbm, sink_ref),
-        local(conv_hbm, conv_ref),
+        local(trig_hbm.at[pl.ds(pl.multiple_of(z * plane, plane), plane)], trig, 6),
+        local(qgain_hbm, qgain_ref, 7),
+        local(kgain_hbm, kgain_ref, 8),
+        local(sink_hbm, sink_ref, 9),
+        local(conv_hbm, conv_ref, 10),
     ]
 
     with scope("barrier"):
@@ -304,7 +293,7 @@
         return win.at[s, 0:core] if kind == 0 else win.at[s, core : core + 3 * cr]
 
     def hop(kind, s, sends, peer):
-        return remote(chunk(kind, s), chunk(kind, s), sends.at[kind, s], w_recv.at[kind, s], peer)
+        return remote(chunk(kind, s), chunk(kind, s), sends.at[kind], w_recv.at[kind, s], peer)
 
     def send_m(kind, s):
         hop(kind, s, m_send, m_peer).start()
@@ -373,43 +362,49 @@
             return ref.at[block]
         return ref.at[block, half * rows // 2 : (half + 1) * rows // 2]
 
-    def tok_hop(block, half, slot, peer):
+    def tok_hop(block, half, place, peer):
         here = part(normed, block, half)
-        return remote(here, here, tok_send.at[slot], tok_recv.at[half, block], peer)
-
-    def end_tok(block, half, slot):
+        return remote(here, here, tok_send.at[0], tok_recv.at[place], peer)
+
+    def end_tok(block, half, place):
         return remote(
-            part(normed, block, half), part(normed2, block, half), tok2_send.at[slot],
-            tok2_recv.at[half, block], m_peer,
+            part(normed, block, half), part(normed2, block, half), tok2_send.at[0],
+            tok2_recv.at[place], m_peer,
         )
 
-    def tok2_hop(block, half, slot, peer):
-        here = part(normed2, block, half)
-        return remote(here, here, tok2_send.at[slot], tok2_recv.at[half, block], peer)
-
-    tok_copies = []
-
-    def tok_go(block, half, peer):
-        copy = tok_hop(block, half, len(tok_copies), peer)
-        copy.start()
-        tok_copies.append(copy)
-
-    def tok_wait(block, half):
-        tok_hop(block, half, 0, x_peer).wait_recv()
-
-    def tok2_wait(block, half):
-        tok2_hop(block, half, 0, x_peer).wait_recv()
+    def tok2_hop(block, place, peer):
+        return remote(
+            normed2.at[block], normed2.at[block], tok2_send.at[0], tok2_recv.at[place], peer
+        )
+
+    def quad(yy, xx):
+        return 2 * yy + xx
+
+    def tok_go(block, half, place, peer):
+        tok_hop(block, half, place, peer).start()
+
+    def tok_wait(block, half, place):
+        tok_hop(block, half, place, x_peer).wait_recv()
+
+    def tok2_wait(block, place):
+        tok2_hop(block, place, x_peer).wait_recv()
+
+    def tok_share(block, yy, xx):
+        tok_go(block, 2, 6 + quad(yy, xx), c_peer)
+
+    def tok2_share(block, yy, xx):
+        tok2_hop(block, 4 + quad(yy, xx), c_peer).start()
 
     @pl.when(is_end)
     def _():
-        end_tok(own_block, 0, 6).start()
-
-    tok_go(own_block, 1, x_peer)
-    tok_go(own_block, 0, y_peer)
-    tok_go(own_block, 0, x_peer)
-    tok_go(own_block, 1, y_peer)
+        end_tok(own_block, 0, 0).start()
+
+    tok_go(own_block, 1, 1, x_peer)
+    tok_go(own_block, 0, 2, y_peer)
+    tok_go(own_block, 0, 0, x_peer)
+    tok_go(own_block, 1, 3, y_peer)
     y_hop(1).start()
-    tok_go(own_block, 2, c_peer)
+    tok_share(own_block, y, x)
 
     with scope("c_mate"):
         take(0, s_mate)
@@ -425,18 +420,18 @@
 
         @pl.when(is_end)
         def _():
-            end_tok(own_block, 1, 7).start()
+            end_tok(own_block, 1, 0).start()
             send_m(1, s_own)
 
     with scope("tok_xy"):
-        tok_wait(xb, 1)
-        tok_go(xb, 1, y_peer)
-        tok_wait(yb, 0)
-        tok_go(yb, 0, x_peer)
-        tok_wait(xb, 0)
-        tok_go(xb, 2, c_peer)
-        tok_wait(yb, 1)
-        tok_go(yb, 2, c_peer)
+        tok_wait(xb, 1, 1)
+        tok_go(xb, 1, 5, y_peer)
+        tok_wait(yb, 0, 2)
+        tok_go(yb, 0, 4, x_peer)
+        tok_wait(xb, 0, 0)
+        tok_share(xb, y, 1 - x)
+        tok_wait(yb, 1, 3)
+        tok_share(yb, 1 - y, x)
 
     with scope("c_fwd"):
         @pl.when(inner)
@@ -450,10 +445,9 @@
         @pl.when(inner)
         def _():
             tok2_wait(own_block, 0)
-            tok2_wait(own_block, 1)
-            tok2_hop(own_block, 2, 0, x_peer).start()
-            tok2_hop(own_block, 2, 1, y_peer).start()
-            tok2_hop(own_block, 2, 2, c_peer).start()
+            tok2_hop(own_block, 2, x_peer).start()
+            tok2_hop(own_block, 3, y_peer).start()
+            tok2_share(own_block, y, x)
 
     y_hop(2).start()
     y_hop(3).start()
@@ -475,14 +469,13 @@
             send_e(0, second_of(far))
 
     with scope("tok_db"):
-        tok_wait(db, 0)
-        tok_wait(db, 1)
-        tok_go(db, 2, c_peer)
+        tok_wait(db, 0, 4)
+        tok_wait(db, 1, 5)
+        tok_share(db, 1 - y, 1 - x)
 
         @pl.when(is_end)
         def _():
-            end_tok(db, 0, 8).start()
-            end_tok(db, 1, 9).start()
+            end_tok(db, 2, 1).start()
 
     with scope("v_near1"):
         @pl.when(inner)
@@ -493,7 +486,7 @@
     with scope("tok_rest"):
         for yy in range(2):
             for xx in range(2):
-                tok_wait(block_of(yy, xx, 1 - c), 2)
+                tok_wait(block_of(yy, xx, 1 - c), 2, 6 + quad(yy, xx))
 
     def columns(s):
         return pl.ds(pl.multiple_of(s * depth, depth), depth)
@@ -602,7 +595,7 @@
         @pl.when(inner)
         def _():
             tok2_wait(xb, 2)
-            tok2_hop(xb, 2, 3, c_peer).start()
+            tok2_share(xb, y, 1 - x)
 
     span = BLOCK + 2 * WINDOW
     total = plane * line
@@ -643,8 +636,8 @@
     with scope("tok2_yb"):
         @pl.when(inner)
         def _():
-            tok2_wait(yb, 2)
-            tok2_hop(yb, 2, 4, c_peer).start()
+            tok2_wait(yb, 3)
+            tok2_share(yb, 1 - y, x)
 
     with scope("v_near2"):
         @pl.when(inner)
@@ -677,9 +670,8 @@
     with scope("tok2_db"):
         @pl.when(inner)
         def _():
-            tok2_wait(db, 0)
             tok2_wait(db, 1)
-            tok2_hop(db, 2, 5, c_peer).start()
+            tok2_share(db, 1 - y, 1 - x)
 
     def attend_edges():
         with scope("rim_wait"):
@@ -726,7 +718,7 @@
         with scope("tok2_rest"):
             for yy in range(2):
                 for xx in range(2):
-                    tok2_wait(block_of(yy, xx, 1 - c), 2)
+                    tok2_wait(block_of(yy, xx, 1 - c), 4 + quad(yy, xx))
 
         with scope("help_dots"):
             early_dots(normed2, acc2, slice(0, 3 * cr), conv_rows, 3)
@@ -801,12 +793,9 @@
 
     mine_rows = jnp.concatenate(group(c), axis=0)
     other_rows = jnp.concatenate(group(1 - c), axis=0)
-    rs_copies = []
-
-    def send_rs(src, dst, stage_id, s, peer):
-        copy = remote(src, dst, rs_send.at[stage_id, s], rs_recv.at[stage_id, s], peer)
-        copy.start()
-        rs_copies.append(copy)
+
+    def rs_hop(src, dst, stage_id, s, peer):
+        return remote(src, dst, rs_send.at[stage_id], rs_recv.at[stage_id, s], peer)
 
     def out_take(i):
         s = 2 * sources[i // 2] + i % 2
@@ -822,7 +811,7 @@
         s1[s] = jnp.dot(
             other_rows, weight, preferred_element_type=jnp.float32
         ).astype(jnp.bfloat16).reshape(2, 2, rows, depth)
-        send_rs(s1.at[s], r1.at[s], 0, s, c_peer)
+        rs_hop(s1.at[s], r1.at[s], 0, s, c_peer).start()
         keep[s] = jnp.dot(
             mine_rows, weight, preferred_element_type=jnp.float32
         ).reshape(2, 2, rows, depth)
@@ -832,19 +821,15 @@
 
     def stage_b(i):
         s = 2 * sources[i // 2] + i % 2
-        remote(s1.at[s], r1.at[s], rs_send.at[0, s], rs_recv.at[0, s], c_peer).wait_recv()
+        rs_hop(s1.at[s], r1.at[s], 0, s, c_peer).wait_recv()
         for j, (yy, xx, peer) in enumerate(corners):
             s2[s, j] = (keep[s, yy, xx] + r1[s, yy, xx].astype(jnp.float32)).astype(jnp.bfloat16)
-            send_rs(s2.at[s, j], r2.at[s, j], 1 + j, s, peer)
+            rs_hop(s2.at[s, j], r2.at[s, j], 1, s, peer).start()
 
     def stage_d(i):
         s = 2 * sources[i // 2] + i % 2
         piece = keep[s, y, x] + r1[s, y, x].astype(jnp.float32)
-        for j in (1, 2, 0):
-            peer = corners[j][2]
-            remote(
-                s2.at[s, j], r2.at[s, j], rs_send.at[1 + j, s], rs_recv.at[1 + j, s], peer
-            ).wait_recv()
+        rs_hop(s2.at[s], r2.at[s], 1, s, d_peer).wait_recv()
         for j in range(3):
             piece = piece + r2[s, j].astype(jnp.float32)
         out_ref[:, columns(s)] = piece.astype(jnp.bfloat16)
@@ -873,11 +858,22 @@
                 else:
                     stage_d(i)
 
+    def sent(ref, send):
+        remote(ref, ref, send, w_recv.at[0, 0], m_peer).wait_send()
+
+    def chunks_sent(kind, count, sends):
+        if kind > 1:
+            ref = wout.at[0:count, 0:qr] if kind == 2 else wout.at[0:count, qr : qr + cr]
+        else:
+            ref = win.at[0:count, 0:core] if kind == 0 else win.at[0:count, core : core + 3 * cr]
+        sent(ref, sends.at[kind])
+
     with scope("sends"):
         for kind in range(4):
             y_hop(kind).wait_send()
-        for copy in tok_copies + rs_copies:
-            copy.wait_send()
+        sent(normed.at[0:7], tok_send.at[0])
+        sent(s1, rs_send.at[0])
+        sent(s2, rs_send.at[1])
 
         @pl.when(has_up)
         def _():
@@ -887,27 +883,20 @@
         def _():
             rim_down.wait_send()
 
-        for kind in range(4):
-            for half in range(2):
-                hop(kind, 2 * z + half, m_send, m_peer).wait_send()
-
         @pl.when(is_end)
         def _():
-            for half in range(2):
-                end_tok(own_block, half, 6 + half).wait_send()
-                end_tok(db, half, 8 + half).wait_send()
-
-        @pl.when(inner)
-        def _():
-            for slot in range(6):
-                tok2_hop(own_block, 2, slot, x_peer).wait_send()
+            sent(normed.at[0:2], tok2_send.at[0])
+            for kind in range(4):
+                chunks_sent(kind, 2, m_send)
+
+        @pl.when(inner)
+        def _():
+            sent(normed2.at[0:6], tok2_send.at[0])
             g_copy.wait_send()
-            for half in range(2):
-                for kind in range(4):
-                    hop(kind, 2 * near + half, m_send, m_peer).wait_send()
-                for source in (z, mid, far):
-                    for kind in (0, 2, 3):
-                        hop(kind, 2 * source + half, e_send, e_peer).wait_send()
+            for kind in range(4):
+                chunks_sent(kind, 4, m_send)
+            for kind in (0, 2, 3):
+                chunks_sent(kind, 6, e_send)
 
         @pl.when(low_inner)
         def _():
@@ -940,8 +929,7 @@
     fan = qr + 2 * kr + 3 * cr
     plane = 8 * rows
     dims = dict(line=line, rows=rows, depth=depth, qr=qr, kr=kr, cr=cr)
-    vm = pl.BlockSpec(memory_space=pltpu.VMEM)
-    hb = pl.BlockSpec(memory_space=pl.ANY)
+    hb = pl.BlockSpec(memory_space=pltpu.HBM)
     bf16, f32 = jnp.bfloat16, jnp.float32
     dma = pltpu.SemaphoreType.DMA
     n = sp_count
@@ -973,26 +961,26 @@
         pltpu.VMEM((n, 2, 2, rows, depth), bf16),
         pltpu.VMEM((n, 3, rows, depth), bf16),
         pltpu.VMEM((n, 3, rows, depth), bf16),
-        dma((23,)), dma((4,)), dma((4, n)), dma((4, n)), dma((4, n)),
-        dma((10,)), dma((3, 8)), dma((10,)), dma((3, 8)), dma((2,)), dma((2,)), dma((2,)), dma((2,)),
-        dma((1,)), dma((1,)), dma((4, n)), dma((4, n)),
+        dma((11,)), dma((4,)), dma((4, n)), dma((4,)), dma((4,)),
+        dma((1,)), dma((10,)), dma((1,)), dma((8,)), dma((2,)), dma((2,)), dma((2,)), dma((2,)),
+        dma((1,)), dma((1,)), dma((2,)), dma((2, n)),
     ]
     taps = conv_weight.reshape(3, 2, cr).transpose(1, 0, 2)
     return pl.pallas_call(
         functools.partial(fused_kernel, dims),
         out_shape=jax.ShapeDtypeStruct((rows, width), bf16),
         in_specs=[hb] * 15,
-        out_specs=vm,
+        out_specs=pl.BlockSpec(memory_space=pltpu.VMEM),
         scratch_shapes=scratch,
         compiler_params=pltpu.CompilerParams(
-            collective_id=0, has_side_effects=True, vmem_limit_bytes=56 * 1024 * 1024
+            collective_id=0, has_side_effects=True, vmem_limit_bytes=32 * 1024 * 1024
         ),
-    )(
+    )(*(pltpu.with_memory_space_constraint(array, pltpu.HBM) for array in (
         tokens, norm_gain[None, :], query_weight, key_weight, value_weight, gate_weight,
         left_weight, input_weight, query_gain[None, :],
         key_gain[None, :], sink_logit[None, :], taps, out_attention, out_conv,
         jnp.asarray(trig_table(plane * line)),
-    )
+    )))
 
 
 def local_device(*args):

time: 62.6 us -> 59.3 us (0.947)
  Pallas kernels: 60.7 us -> 58.4 us
  local copies, waits for them, and re-layouts: 1.67 us -> 0.71 us
    pallas_call x1, Pallas kernels: 60.7 us -> 58.4 us  [fused_device(): pl.pallas_call(functools.partial(fused_kernel, dims), out_shape=jax.Shape...]
    unnamed x1, local copies, waits for them, and re-layouts: 1.67 us -> 0.71 us
where the time goes in v3:
time: 59.3 us; the launch traced here: 59.1 us
  Pallas kernels  58.4 us (98%)
  local copies, waits for them, and re-layouts  0.71 us (1%)
    pallas_call x1, Pallas kernels, fused_device(): pl.pallas_call(functools.partial(fused_kernel, dims), out_shape=jax.Shape...  58.4 us

profile of v3, /device:TPU:0, one launch (start us, length us, event | category | flops | bytes accessed | tf_op | source)
XLA Modules:
  0.0 59.1 jit_solution(340389090080975934)
XLA Ops:
  0.0 58.4 %shard_map.145 = bf16[64,2048]{1,0:T(8,128)(2,1)S(1)} custom-call(bf16[64,2048]{1,0:T(8,128)(2,1)} %tok_hbm.1, f32[1,2048]{1,0:T(1,128)} %bitcast.7, bf16[256,256]{1,0:T(8,128)(2,1)} %q_hbm.1, bf16[64,256]{1,0:T(8,128)(2,1)} %k_hbm.1, bf16[64,256]{1,0:T(8,128)(2,1)} %v_hbm.1, bf16[256,256]{1,0:T(8,128)(2,1)} %g_hbm.1, bf16[256,256]{1,0:T(8,128)(2,1)} %l_hbm.1, ...), custom_call_target="tpu_custom_call" | custom-call | tf_op jit(solution)/shard_map/pallas_call | solution.py:969
  58.4 0.7 %copy.17 = bf16[64,2048]{1,0:T(8,128)(2,1)} copy(bf16[64,2048]{1,0:T(8,128)(2,1)S(1)} %shard_map.145) | data formatting | bytes 524288

commit v4 on v3

--- a/solution.py
+++ b/solution.py
@@ -203,11 +203,11 @@
     tok_hbm, gain_hbm, q_hbm, k_hbm, v_hbm, g_hbm, l_hbm, i_hbm,
     qgain_hbm, kgain_hbm, sink_hbm, conv_hbm, oa_hbm, oc_hbm, trig_hbm,
     out_ref,
-    gain_ref, qgain_ref, kgain_ref, sink_ref, conv_ref, tok, trig, stage, ostage, win, wout, normed, normed2, acc, acc2, rim, prod, prod2, mix_a, mix_c, gated2,
+    gain_ref, qgain_ref, kgain_ref, sink_ref, conv_ref, tok, trig, stage, ostage, win, wout, normed, normed2, acc, acc2, keys, prod, prod2, mix_a, mix_c, gated2,
     qrot,
     keep, s1, r1, s2, r2,
     local_sem, y_send, w_recv, m_send, e_send,
-    tok_send, tok_recv, tok2_send, tok2_recv, rim_send, rim_recv, prod_send, prod_recv, g_send, g_recv,
+    tok_send, tok_recv, tok2_send, tok2_recv, rim_send, rim_recv, kv_send, kv_recv, prod_send, prod_recv, g_send, g_recv,
     rs_send, rs_recv,
 ):
     scope = jax.named_scope
@@ -236,7 +236,7 @@
     s_own = sp
     s_mate = 2 * z + 1 - y
     plane = 8 * rows
-    core = qr + 2 * kr
+    core = qr + kr
 
     barrier = pltpu.get_barrier_semaphore()
     for peer in (y_peer, x_peer, c_peer, m_peer):
@@ -254,8 +254,15 @@
     def in_pieces(which, dst, place):
         q0, c0 = pl.multiple_of(which * qr, qr), pl.multiple_of(which * cr, cr)
         local(q_hbm.at[pl.ds(q0, qr)], dst.at[0:qr], place)
-        local(k_hbm, dst.at[qr : qr + kr], place)
-        local(v_hbm, dst.at[qr + kr : core], place)
+
+        @pl.when(which == 0)
+        def _():
+            local(k_hbm, dst.at[qr:core], place)
+
+        @pl.when(which == 1)
+        def _():
+            local(v_hbm, dst.at[qr:core], place)
+
         for turn, ref in enumerate((g_hbm, l_hbm, i_hbm)):
             lo = core + turn * cr
             local(ref.at[pl.ds(c0, cr)], dst.at[lo : lo + cr], place)
@@ -441,6 +448,10 @@
             take(0, second_of(near))
             send_m(0, second_of(near))
 
+        @pl.when(inner & (c == 1))
+        def _():
+            out_send(s_own, send_m)
+
     with scope("tok2_own"):
         @pl.when(inner)
         def _():
@@ -482,6 +493,10 @@
         def _():
             take(1, first_of(near))
             send_m(1, first_of(near))
+
+        @pl.when(inner & (c == 1))
+        def _():
+            out_hop(first_of(mid), send_e)
 
     with scope("tok_rest"):
         for yy in range(2):
@@ -504,6 +519,7 @@
         into[:, cols] = total
 
     conv_rows = slice(core, core + 3 * cr)
+    conv_cols = slice(2 * qr, 2 * qr + 3 * cr)
 
     def early_dots(tokens, into, cols, weight_rows, count):
         plane_dots(tokens, into, cols, weight_rows, z, False)
@@ -544,12 +560,13 @@
         def bf(v):
             return v.astype(jnp.bfloat16).astype(jnp.float32)
 
-        kv = bf(acc[:, qr : 2 * qr])
-        ksq = jnp.sum(jnp.where(low, kv * kv, 0.0), axis=-1, keepdims=True) / HEAD_DIM
+        kv = jnp.where(low, bf(acc[:, qr : 2 * qr]), 0.0)
+        ksq = jnp.sum(kv * kv, axis=-1, keepdims=True) / HEAD_DIM
         kgain = jnp.concatenate([kgain_ref[...], kgain_ref[...]], axis=1)
         kn = kv * lax.rsqrt(ksq + EPS) * kgain
         krot = rot(kn)
-        rim[WINDOW : WINDOW + plane, :] = jnp.where(low, krot, kv).astype(jnp.bfloat16)
+        keyed = jnp.where(y == 0, jnp.where(low, krot, 0.0), kv)
+        keys[y, WINDOW : WINDOW + plane, :] = keyed.astype(jnp.bfloat16)
 
     bottom = pl.ds(WINDOW, WINDOW)
     top = pl.ds(plane, WINDOW)
@@ -557,9 +574,12 @@
     down = (jnp.maximum(2 * (z - 1) + y, 0), tp)
     has_up = z < line - 1
     has_down = z > 0
-    rim_up = remote(rim.at[top], rim.at[pl.ds(0, WINDOW)], rim_send.at[0], rim_recv.at[0], up)
+    rim_up = remote(
+        keys.at[y, top], keys.at[y, pl.ds(0, WINDOW)], rim_send.at[0], rim_recv.at[0], up
+    )
     rim_down = remote(
-        rim.at[bottom], rim.at[pl.ds(WINDOW + plane, WINDOW)], rim_send.at[1], rim_recv.at[1], down
+        keys.at[y, bottom], keys.at[y, pl.ds(WINDOW + plane, WINDOW)], rim_send.at[1],
+        rim_recv.at[1], down,
     )
 
     @pl.when(has_up)
@@ -570,15 +590,21 @@
     def _():
         rim_down.start()
 
-    zero_rim = jnp.zeros((WINDOW, qr), jnp.bfloat16)
+    def kv_hop(place):
+        begin, size = ((WINDOW, plane), (0, WINDOW), (WINDOW + plane, WINDOW))[place]
+        here = keys.at[y, pl.ds(begin, size)]
+        return remote(here, here, kv_send.at[place], kv_recv.at[place], y_peer)
+
+    kv_hop(0).start()
+    zero_rim = jnp.zeros((2, WINDOW, qr), jnp.bfloat16)
 
     @pl.when(z == 0)
     def _():
-        rim[0:WINDOW] = zero_rim
+        keys[:, 0:WINDOW] = zero_rim
 
     @pl.when(z == line - 1)
     def _():
-        rim[WINDOW + plane :] = zero_rim
+        keys[:, WINDOW + plane :] = zero_rim
 
     with scope("rotq"):
         qv = bf(acc[:, 0:qr])
@@ -602,10 +628,11 @@
 
     def att_block(block):
         begin = pl.multiple_of(block * BLOCK, BLOCK)
-        kvb = rim[pl.ds(begin, span), :]
+        keyed = keys[0, pl.ds(begin, span), :]
+        valued = keys[1, pl.ds(begin, span), :]
         qb = qrot[:, pl.ds(begin, BLOCK), :].reshape(2 * BLOCK, qr)
         scores = lax.dot_general(
-            qb, kvb, (((1,), (1,)), ((), ())), preferred_element_type=jnp.float32
+            qb, keyed, (((1,), (1,)), ((), ())), preferred_element_type=jnp.float32
         ) * HEAD_DIM ** (-0.5)
         row = lax.broadcasted_iota(jnp.int32, (2 * BLOCK, span), 0)
         col = lax.broadcasted_iota(jnp.int32, (2 * BLOCK, span), 1)
@@ -619,9 +646,9 @@
         expo = jnp.exp(scores - peak)
         denom = jnp.sum(expo, axis=-1, keepdims=True) + jnp.exp(sink - peak)
         weights = (expo / denom).astype(jnp.bfloat16)
-        o = jnp.dot(weights, kvb, preferred_element_type=jnp.float32)
+        o = jnp.dot(weights, valued, preferred_element_type=jnp.float32)
         low_b = lax.broadcasted_iota(jnp.int32, (BLOCK, qr), 1) < HEAD_DIM
-        both = jnp.where(low_b, pltpu.roll(o[:BLOCK], HEAD_DIM, 1), o[BLOCK:])
+        both = jnp.where(low_b, o[:BLOCK], pltpu.roll(o[BLOCK:], HEAD_DIM, 1))
         mix_a[pl.ds(begin, BLOCK), :] = both.astype(jnp.bfloat16)
 
     nblocks = plane // BLOCK
@@ -630,8 +657,15 @@
         att_block(block)
         return carry
 
-    with scope("att_in"):
-        lax.fori_loop(1, nblocks - 1, att_inner, 0)
+    with scope("v_near2"):
+        @pl.when(inner)
+        def _():
+            take(1, second_of(near))
+            send_m(1, second_of(near))
+
+        @pl.when(inner & (c == 0))
+        def _():
+            out_send(s_own, send_m)
 
     with scope("tok2_yb"):
         @pl.when(inner)
@@ -639,23 +673,6 @@
             tok2_wait(yb, 3)
             tok2_share(yb, 1 - y, x)
 
-    with scope("v_near2"):
-        @pl.when(inner)
-        def _():
-            take(1, second_of(near))
-            send_m(1, second_of(near))
-
-    with scope("o_mate"):
-        @pl.when(is_end)
-        def _():
-            out_send(s_own, send_m)
-            out_hop(s_mate, send_m)
-
-        @pl.when(inner)
-        def _():
-            out_send(s_own, send_m)
-            out_hop(s_mate, send_e)
-
     with scope("v_mid"):
         @pl.when(inner)
         def _():
@@ -665,23 +682,59 @@
     with scope("v_dots"):
         @pl.when(inner)
         def _():
-            early_dots(normed, acc, conv_rows, conv_rows, 3)
-
-    with scope("tok2_db"):
-        @pl.when(inner)
-        def _():
-            tok2_wait(db, 1)
-            tok2_share(db, 1 - y, 1 - x)
-
-    def attend_edges():
+            early_dots(normed, acc, conv_cols, conv_rows, 3)
+
+    def share_rims():
         with scope("rim_wait"):
             @pl.when(has_down)
             def _():
                 rim_up.wait_recv()
+                kv_hop(1).start()
 
             @pl.when(has_up)
             def _():
                 rim_down.wait_recv()
+                kv_hop(2).start()
+
+    with scope("tok2_db"):
+        @pl.when(inner)
+        def _():
+            tok2_wait(db, 1)
+            tok2_share(db, 1 - y, 1 - x)
+
+    with scope("o_mate"):
+        @pl.when(is_end)
+        def _():
+            out_send(s_own, send_m)
+            out_hop(s_mate, send_m)
+
+    share_rims()
+
+    with scope("o_mate"):
+        @pl.when(inner)
+        def _():
+            out_hop(s_mate, send_m, send_e)
+
+    def attend():
+        with scope("kv_wait"):
+            kv_hop(0).wait_recv()
+
+        with scope("att_in"):
+            lax.fori_loop(1, nblocks - 1, att_inner, 0)
+
+        with scope("o_fwd"):
+            @pl.when(inner)
+            def _():
+                out_hop(second_of(mid), send_e)
+
+        with scope("kv_rims"):
+            @pl.when(has_down)
+            def _():
+                kv_hop(1).wait_recv()
+
+            @pl.when(has_up)
+            def _():
+                kv_hop(2).wait_recv()
 
         with scope("att_out"):
             def att_outer(k, carry):
@@ -693,7 +746,7 @@
     pad = 16
     zero_pad = jnp.zeros((pad, cr), jnp.bfloat16)
     taps = conv_ref[y]
-    base = core
+    base = 2 * qr
 
     def convolve(ref, gate):
         p = ref[...].astype(jnp.float32)
@@ -727,7 +780,7 @@
             for s in (first_of(far), second_of(far)):
                 take(1, s)
             plane_dots(normed2, acc2, slice(0, 3 * cr), conv_rows, far, True)
-            plane_dots(normed, acc, conv_rows, conv_rows, far, True)
+            plane_dots(normed, acc, conv_cols, conv_rows, far, True)
 
         with scope("prod"):
             left = bf(acc[:, base + cr : base + 2 * cr])
@@ -742,7 +795,6 @@
             def _():
                 prod_down.start()
 
-            out_send(s_mate, send_m)
             out_hop(first_of(near), send_m)
 
             prod2[pad : pad + plane] = (
@@ -764,11 +816,13 @@
             gated2[...] = convolve(prod2, bf(acc2[:, 0:cr]))
             g_copy.start()
 
-        attend_edges()
-
-        with scope("o_fwd"):
+            @pl.when(c == 0)
+            def _():
+                out_hop(first_of(mid), send_e)
+
             out_hop(second_of(near), send_m)
-            out_hop(first_of(mid), send_e)
+
+        attend()
 
         with scope("prod_wait"):
             @pl.when(low_inner)
@@ -783,7 +837,7 @@
 
     @pl.when(is_end)
     def _():
-        attend_edges()
+        attend()
         with scope("g_wait"):
             g_copy.wait_recv()
 
@@ -795,7 +849,7 @@
     other_rows = jnp.concatenate(group(1 - c), axis=0)
 
     def rs_hop(src, dst, stage_id, s, peer):
-        return remote(src, dst, rs_send.at[stage_id], rs_recv.at[stage_id, s], peer)
+        return remote(src, dst, rs_send.at[min(stage_id, 1)], rs_recv.at[stage_id, s], peer)
 
     def out_take(i):
         s = 2 * sources[i // 2] + i % 2
@@ -819,27 +873,61 @@
     d_peer = (2 * z + 1 - y, 2 * (1 - x) + c)
     corners = ((1 - y, 1 - x, d_peer), (1 - y, x, y_peer), (y, 1 - x, x_peer))
 
+    staged = 4
+
     def stage_b(i):
-        s = 2 * sources[i // 2] + i % 2
+        half = i % 2
+        s = 2 * sources[i // 2] + half
         rs_hop(s1.at[s], r1.at[s], 0, s, c_peer).wait_recv()
-        for j, (yy, xx, peer) in enumerate(corners):
+
+        def put(j, yy, xx):
             s2[s, j] = (keep[s, yy, xx] + r1[s, yy, xx].astype(jnp.float32)).astype(jnp.bfloat16)
-            rs_hop(s2.at[s, j], r2.at[s, j], 1, s, peer).start()
+
+        if i < staged:
+            for j in range(2):
+                put(j, *((1 - y, j) if half == 0 else (j, 1 - x)))
+            pair_hop(s, half).start()
+        else:
+            for j, (yy, xx, peer) in enumerate(corners):
+                put(j, yy, xx)
+                rs_hop(s2.at[s, j], r2.at[s, j], 1, s, peer).start()
+
+    def pair_hop(s, half):
+        peer = y_peer if half == 0 else x_peer
+        return rs_hop(s2.at[s, 0:2], r2.at[s, 0:2], 1, s, peer)
+
+    def last_hop(s, half):
+        peer = x_peer if half == 0 else y_peer
+        return rs_hop(s2.at[s, 2], r2.at[s, 2], 2, s, peer)
+
+    def stage_c(i):
+        half = i % 2
+        s = 2 * sources[i // 2] + half
+        pair_hop(s, half).wait_recv()
+        yy, xx, j = (y, 1 - x, 1 - x) if half == 0 else (1 - y, x, 1 - y)
+        piece = keep[s, yy, xx] + r1[s, yy, xx].astype(jnp.float32)
+        s2[s, 2] = (piece + r2[s, j].astype(jnp.float32)).astype(jnp.bfloat16)
+        last_hop(s, half).start()
 
     def stage_d(i):
-        s = 2 * sources[i // 2] + i % 2
+        half = i % 2
+        s = 2 * sources[i // 2] + half
         piece = keep[s, y, x] + r1[s, y, x].astype(jnp.float32)
-        rs_hop(s2.at[s], r2.at[s], 1, s, d_peer).wait_recv()
-        for j in range(3):
-            piece = piece + r2[s, j].astype(jnp.float32)
+        if i < staged:
+            last_hop(s, half).wait_recv()
+            piece = piece + r2[s, x if half == 0 else y].astype(jnp.float32)
+            piece = piece + r2[s, 2].astype(jnp.float32)
+        else:
+            rs_hop(s2.at[s], r2.at[s], 1, s, d_peer).wait_recv()
+            for j in range(3):
+                piece = piece + r2[s, j].astype(jnp.float32)
         out_ref[:, columns(s)] = piece.astype(jnp.bfloat16)
 
     order = (
-        ("a", (0, 1)), ("f", (5,)), ("b", (0,)), ("a", (2,)), ("b", (1,)), ("a", (3,)),
-        ("b", (2, 3)), ("w", (4,)), ("a", (4,)), ("f", (6,)), ("b", (4,)),
-        ("w", (5,)), ("a", (5,)), ("b", (5,)), ("f", (7,)), ("w", (6,)), ("a", (6,)), ("b", (6,)),
-        ("d", (0, 1)), ("w", (7,)), ("a", (7,)), ("b", (7,)),
-        ("d", (2, 3, 4, 5, 6, 7)),
+        ("a", (0, 1,)), ("f", (6,)), ("b", (0,)), ("a", (2,)), ("b", (1,)), ("a", (3,)),
+        ("b", (2,)), ("w", (4,)), ("a", (4,)), ("b", (3,)), ("f", (7,)), ("w", (5,)), ("a", (5,)),
+        ("b", (4,)), ("c", (0, 1,)), ("w", (6,)), ("a", (6,)), ("b", (5,)), ("c", (2, 3,)),
+        ("w", (7,)), ("a", (7,)), ("b", (6, 7,)), ("d", (0, 1, 2, 3, 4, 6, 5, 7,)),
     )
 
     for step, places in order:
@@ -855,6 +943,8 @@
                     stage_a(i)
                 elif step == "b":
                     stage_b(i)
+                elif step == "c":
+                    stage_c(i)
                 else:
                     stage_d(i)
 
@@ -875,13 +965,17 @@
         sent(s1, rs_send.at[0])
         sent(s2, rs_send.at[1])
 
+        kv_hop(0).wait_send()
+
         @pl.when(has_up)
         def _():
             rim_up.wait_send()
+            kv_hop(2).wait_send()
 
         @pl.when(has_down)
         def _():
             rim_down.wait_send()
+            kv_hop(1).wait_send()
 
         @pl.when(is_end)
         def _():
@@ -926,7 +1020,7 @@
     qr = query_weight.shape[0] // 2
     kr = key_weight.shape[0]
     cr = gate_weight.shape[0] // 2
-    fan = qr + 2 * kr + 3 * cr
+    fan = qr + kr + 3 * cr
     plane = 8 * rows
     dims = dict(line=line, rows=rows, depth=depth, qr=qr, kr=kr, cr=cr)
     hb = pl.BlockSpec(memory_space=pltpu.HBM)
@@ -947,9 +1041,9 @@
         pltpu.VMEM((n, qr + cr, depth), bf16),
         pltpu.VMEM((8, rows, width), bf16),
         pltpu.VMEM((8, rows, width), bf16),
-        pltpu.VMEM((plane, fan), f32),
+        pltpu.VMEM((plane, 2 * qr + 3 * cr), f32),
         pltpu.VMEM((plane, 3 * cr), f32),
-        pltpu.VMEM((plane + 2 * WINDOW, qr), bf16),
+        pltpu.VMEM((2, plane + 2 * WINDOW, qr), bf16),
         pltpu.VMEM((plane + 32, cr), bf16),
         pltpu.VMEM((plane + 32, cr), bf16),
         pltpu.VMEM((plane, qr), bf16),
@@ -962,8 +1056,9 @@
         pltpu.VMEM((n, 3, rows, depth), bf16),
         pltpu.VMEM((n, 3, rows, depth), bf16),
         dma((11,)), dma((4,)), dma((4, n)), dma((4,)), dma((4,)),
-        dma((1,)), dma((10,)), dma((1,)), dma((8,)), dma((2,)), dma((2,)), dma((2,)), dma((2,)),
-        dma((1,)), dma((1,)), dma((2,)), dma((2, n)),
+        dma((1,)), dma((10,)), dma((1,)), dma((8,)), dma((2,)), dma((2,)), dma((3,)), dma((3,)),
+        dma((2,)), dma((2,)),
+        dma((1,)), dma((1,)), dma((2,)), dma((3, n)),
     ]
     taps = conv_weight.reshape(3, 2, cr).transpose(1, 0, 2)
     return pl.pallas_call(

time: 59.3 us -> 57.8 us (0.975)
  Pallas kernels: 58.4 us -> 56.9 us
    pallas_call x1, Pallas kernels: 58.4 us -> 56.9 us  [fused_device(): pl.pallas_call(functools.partial(fused_kernel, dims), out_shape=jax.Shape...]
where the time goes in v4:
time: 57.8 us; the launch traced here: 57.6 us
  Pallas kernels  56.9 us (98%)
  local copies, waits for them, and re-layouts  0.71 us (1%)
    pallas_call x1, Pallas kernels, fused_device(): pl.pallas_call(functools.partial(fused_kernel, dims), out_shape=jax.Shape...  56.9 us

profile of v4, /device:TPU:0, one launch (start us, length us, event | category | flops | bytes accessed | tf_op | source)
XLA Modules:
  0.0 57.6 jit_solution(6395127582699276808)
XLA Ops:
  0.0 56.9 %shard_map.145 = bf16[64,2048]{1,0:T(8,128)(2,1)S(1)} custom-call(bf16[64,2048]{1,0:T(8,128)(2,1)} %tok_hbm.1, f32[1,2048]{1,0:T(1,128)} %bitcast.7, bf16[256,256]{1,0:T(8,128)(2,1)} %q_hbm.1, bf16[64,256]{1,0:T(8,128)(2,1)} %k_hbm.1, bf16[64,256]{1,0:T(8,128)(2,1)} %v_hbm.1, bf16[256,256]{1,0:T(8,128)(2,1)} %g_hbm.1, bf16[256,256]{1,0:T(8,128)(2,1)} %l_hbm.1, ...), custom_call_target="tpu_custom_call" | custom-call | tf_op jit(solution)/shard_map/pallas_call | solution.py:1064
  56.9 0.7 %copy.17 = bf16[64,2048]{1,0:T(8,128)(2,1)} copy(bf16[64,2048]{1,0:T(8,128)(2,1)S(1)} %shard_map.145) | data formatting | bytes 524288

commit v5 on v4

--- a/solution.py
+++ b/solution.py
@@ -448,7 +448,7 @@
             take(0, second_of(near))
             send_m(0, second_of(near))
 
-        @pl.when(inner & (c == 1))
+        @pl.when(inner)
         def _():
             out_send(s_own, send_m)
 
@@ -494,7 +494,7 @@
             take(1, first_of(near))
             send_m(1, first_of(near))
 
-        @pl.when(inner & (c == 1))
+        @pl.when(inner)
         def _():
             out_hop(first_of(mid), send_e)
 
@@ -663,10 +663,6 @@
             take(1, second_of(near))
             send_m(1, second_of(near))
 
-        @pl.when(inner & (c == 0))
-        def _():
-            out_send(s_own, send_m)
-
     with scope("tok2_yb"):
         @pl.when(inner)
         def _():
@@ -795,7 +791,7 @@
             def _():
                 prod_down.start()
 
-            out_hop(first_of(near), send_m)
+            out_hop(2 * near, send_m)
 
             prod2[pad : pad + plane] = (
                 bf(acc2[:, cr : 2 * cr]) * bf(acc2[:, 2 * cr : 3 * cr])
@@ -816,11 +812,7 @@
             gated2[...] = convolve(prod2, bf(acc2[:, 0:cr]))
             g_copy.start()
 
-            @pl.when(c == 0)
-            def _():
-                out_hop(first_of(mid), send_e)
-
-            out_hop(second_of(near), send_m)
+            out_hop(2 * near + 1, send_m)
 
         attend()
 
@@ -856,8 +848,7 @@
         out_hop(s)
 
     def out_forward(i):
-        source = sources[i // 2]
-        out_hop(first_of(source) if i % 2 == 0 else second_of(source), send_e)
+        out_hop(2 * sources[i // 2] + i % 2, send_e)
 
     def stage_a(i):
         s = 2 * sources[i // 2] + i % 2
@@ -873,7 +864,7 @@
     d_peer = (2 * z + 1 - y, 2 * (1 - x) + c)
     corners = ((1 - y, 1 - x, d_peer), (1 - y, x, y_peer), (y, 1 - x, x_peer))
 
-    staged = 4
+    staged = 6
 
     def stage_b(i):
         half = i % 2
@@ -927,7 +918,8 @@
         ("a", (0, 1,)), ("f", (6,)), ("b", (0,)), ("a", (2,)), ("b", (1,)), ("a", (3,)),
         ("b", (2,)), ("w", (4,)), ("a", (4,)), ("b", (3,)), ("f", (7,)), ("w", (5,)), ("a", (5,)),
         ("b", (4,)), ("c", (0, 1,)), ("w", (6,)), ("a", (6,)), ("b", (5,)), ("c", (2, 3,)),
-        ("w", (7,)), ("a", (7,)), ("b", (6, 7,)), ("d", (0, 1, 2, 3, 4, 6, 5, 7,)),
+        ("w", (7,)), ("a", (7,)), ("b", (6, 7,)), ("c", (4, 5,)),
+        ("d", (0, 1, 2, 3, 4, 6, 5, 7,)),
     )
 
     for step, places in order:

time: 57.8 us -> 56.6 us (0.979)
  Pallas kernels: 56.9 us -> 55.7 us
    pallas_call x1, Pallas kernels: 56.9 us -> 55.7 us  [fused_device(): pl.pallas_call(functools.partial(fused_kernel, dims), out_shape=jax.Shape...]
where the time goes in v5:
time: 56.6 us; the launch traced here: 56.4 us
  Pallas kernels  55.7 us (98%)
  local copies, waits for them, and re-layouts  0.71 us (1%)
    pallas_call x1, Pallas kernels, fused_device(): pl.pallas_call(functools.partial(fused_kernel, dims), out_shape=jax.Shape...  55.7 us

profile of v5, /device:TPU:0, one launch (start us, length us, event | category | flops | bytes accessed | tf_op | source)
XLA Modules:
  0.0 56.4 jit_solution(2773687167448475220)
XLA Ops:
  0.0 55.7 %shard_map.145 = bf16[64,2048]{1,0:T(8,128)(2,1)S(1)} custom-call(bf16[64,2048]{1,0:T(8,128)(2,1)} %tok_hbm.1, f32[1,2048]{1,0:T(1,128)} %bitcast.7, bf16[256,256]{1,0:T(8,128)(2,1)} %q_hbm.1, bf16[64,256]{1,0:T(8,128)(2,1)} %k_hbm.1, bf16[64,256]{1,0:T(8,128)(2,1)} %v_hbm.1, bf16[256,256]{1,0:T(8,128)(2,1)} %g_hbm.1, bf16[256,256]{1,0:T(8,128)(2,1)} %l_hbm.1, ...), custom_call_target="tpu_custom_call" | custom-call | tf_op jit(solution)/shard_map/pallas_call | solution.py:1056
  55.7 0.7 %copy.17 = bf16[64,2048]{1,0:T(8,128)(2,1)} copy(bf16[64,2048]{1,0:T(8,128)(2,1)S(1)} %shard_map.145) | data formatting | bytes 524288

commit v6 on v5

--- a/solution.py
+++ b/solution.py
@@ -447,10 +447,11 @@
             send_e(0, second_of(mid))
             take(0, second_of(near))
             send_m(0, second_of(near))
-
-        @pl.when(inner)
-        def _():
-            out_send(s_own, send_m)
+            send_m(2, s_own)
+
+        @pl.when(inner & (c == 1))
+        def _():
+            send_m(3, s_own)
 
     with scope("tok2_own"):
         @pl.when(inner)
@@ -496,7 +497,13 @@
 
         @pl.when(inner)
         def _():
-            out_hop(first_of(mid), send_e)
+            take(2, first_of(mid))
+            send_e(2, first_of(mid))
+
+        @pl.when(inner & (c == 1))
+        def _():
+            take(3, first_of(mid))
+            send_e(3, first_of(mid))
 
     with scope("tok_rest"):
         for yy in range(2):
@@ -663,6 +670,11 @@
             take(1, second_of(near))
             send_m(1, second_of(near))
 
+        @pl.when(inner & (c == 0))
+        def _():
+            send_m(3, s_own)
+
+
     with scope("tok2_yb"):
         @pl.when(inner)
         def _():
@@ -722,6 +734,11 @@
             @pl.when(inner)
             def _():
                 out_hop(second_of(mid), send_e)
+
+            @pl.when(inner & (c == 0))
+            def _():
+                take(3, first_of(mid))
+                send_e(3, first_of(mid))
 
         with scope("kv_rims"):
             @pl.when(has_down)

time: 56.6 us -> 56.2 us (level)
  no operation moved by 1% of the time
where the time goes in v6:
time: 56.2 us; the launch traced here: 56.1 us
  Pallas kernels  55.4 us (99%)
  local copies, waits for them, and re-layouts  0.71 us (1%)
    pallas_call x1, Pallas kernels, fused_device(): pl.pallas_call(functools.partial(fused_kernel, dims), out_shape=jax.Shape...  55.4 us

profile of v6, /device:TPU:0, one launch (start us, length us, event | category | flops | bytes accessed | tf_op | source)
XLA Modules:
  0.0 56.1 jit_solution(10290830307009373228)
XLA Ops:
  0.0 55.4 %shard_map.145 = bf16[64,2048]{1,0:T(8,128)(2,1)S(1)} custom-call(bf16[64,2048]{1,0:T(8,128)(2,1)} %tok_hbm.1, f32[1,2048]{1,0:T(1,128)} %bitcast.7, bf16[256,256]{1,0:T(8,128)(2,1)} %q_hbm.1, bf16[64,256]{1,0:T(8,128)(2,1)} %k_hbm.1, bf16[64,256]{1,0:T(8,128)(2,1)} %v_hbm.1, bf16[256,256]{1,0:T(8,128)(2,1)} %g_hbm.1, bf16[256,256]{1,0:T(8,128)(2,1)} %l_hbm.1, ...), custom_call_target="tpu_custom_call" | custom-call | tf_op jit(solution)/shard_map/pallas_call | solution.py:1073
  55.4 0.7 %copy.17 = bf16[64,2048]{1,0:T(8,128)(2,1)} copy(bf16[64,2048]{1,0:T(8,128)(2,1)S(1)} %shard_map.145) | data formatting | bytes 524288
